TPU v7x, 32 devices: a whole 2x2x4 slice. The times are simulated.
32 devices in a mesh: grp: 2 (over y), sp: 4 (over z), tp: 4 (over x, core).
Axes of the slice: x: 2, y: 2, z: 4, core: 2. Of those that a mesh axis runs over, the one named last changes fastest.
Arguments:
- query_rows: bfloat16 [4096, 512], P(('grp', 'sp'), 'tp'), parts along dimension 0, may hold values from -12 to 12
- key_rows: bfloat16 [4096, 512], P(('grp', 'sp'), 'tp'), parts along dimension 0, may hold values from -12 to 12
- value_rows: bfloat16 [4096, 512], P(('grp', 'sp'), 'tp'), parts along dimension 0, may hold values from -12 to 12
- residual: bfloat16 [4096, 2048], P(('grp', 'sp', 'tp')), parts along dimension 0, may hold values from -6 to 6
- output_weight: bfloat16 [512, 2048], P('tp'), may hold values from -0.25 to 0.25
- first_gain: float32 [2048], replicated, may hold values from 0.1 to 1.9
- first_bias: float32 [2048], replicated, may hold values from -3 to 3
- expert_ids: int32 [4096, 4], P(('grp', 'sp', 'tp')), parts along dimension 0, may hold values from 0 to 15, all different within a row; in each aligned block of 128 rows (0 to 127, 128 to 255, ...) at most 48 rows name the same one
- expert_share: float32 [4096, 4], P(('grp', 'sp', 'tp')), parts along dimension 0, may hold values from 0.3 to 1.2
- gate_weight: bfloat16 [16, 2048, 256], P(('sp', 'tp')), may hold values from -0.125 to 0.125
- up_weight: bfloat16 [16, 2048, 256], P(('sp', 'tp')), may hold values from -0.125 to 0.125
- down_weight: bfloat16 [16, 256, 2048], P(('sp', 'tp')), may hold values from -0.375 to 0.375
- shared_gate: bfloat16 [2048, 512], replicated, may hold values from -0.125 to 0.125
- shared_up: bfloat16 [2048, 512], replicated, may hold values from -0.125 to 0.125
- shared_down: bfloat16 [512, 2048], replicated, may hold values from -0.25 to 0.25
- second_gain: float32 [2048], replicated, may hold values from 0.1 to 1.9
- second_bias: float32 [2048], replicated, may hold values from -3 to 3
Outputs:
- layer_out: bfloat16 [4096, 2048], P(('grp', 'sp', 'tp')), parts along dimension 0
There are 2 independent parts, one for each index of `grp`. A program takes and returns all parts, laid end to end along the dimension named above; an argument that names none is the same for every part. Nothing has to cross between parts.
Inputs may be any that keep to these rules, and one draw needn't show every extreme that they name: `expert_ids`: each row names 4 different experts. Among the rows of one device (aligned blocks of 128 rows) no expert is named by more than 48 rows, a bound that some block reaches.
All inputs are finite; a program needn't handle non-finite values.
Results may differ from a plain program's by a relative error of at most 0.012.
Values may be sent and summed in bfloat16 or wider, within the bound.
A program may use at most 128 MiB of HBM per device.

v0:
```python
import jax
import jax.numpy as jnp
from jax import lax
from jax.sharding import PartitionSpec as P

HEAD_DIM = 128
KBLK = 128


NORM_EPS = 1e-05


def layer_norm(summed, gains, offset):
    average = jnp.mean(summed, axis=-1, keepdims=True)
    centred = summed - average
    spread = jnp.mean(centred * centred, axis=-1, keepdims=True)
    return centred * lax.rsqrt(spread + NORM_EPS) * gains + offset


def stick_local(query_rows, key_all, value_all, seq_index):
    shard_len = query_rows.shape[0]
    heads_here = query_rows.shape[1] // HEAD_DIM
    step_len = 2 * shard_len
    blocks_per = step_len // KBLK
    scale = HEAD_DIM ** (-0.5)
    queries = query_rows.reshape(shard_len, heads_here, HEAD_DIM)
    query_pos = seq_index * shard_len + jnp.arange(shard_len, dtype=jnp.int32)
    visits = seq_index // 2 + 1
    upper = (jnp.arange(KBLK)[:, None] >= jnp.arange(KBLK)[None, :]).astype(jnp.float32)

    def visit(visit_no, carry):
        summed, behind = carry
        chosen = visits - 1 - visit_no
        first_key = chosen * step_len
        key_block = lax.dynamic_slice_in_dim(key_all, first_key, step_len, 0).reshape(
            step_len, heads_here, HEAD_DIM
        )
        value_block = lax.dynamic_slice_in_dim(value_all, first_key, step_len, 0).reshape(
            blocks_per, KBLK, heads_here, HEAD_DIM
        )
        key_pos = (first_key + jnp.arange(step_len, dtype=jnp.int32)).reshape(blocks_per, KBLK)
        score = (
            jnp.einsum("qhd,khd->qhk", queries, key_block, preferred_element_type=jnp.float32)
            * scale
        )
        score = score.reshape(shard_len, heads_here, blocks_per, KBLK)
        usable = key_pos[None, None, :, :] < query_pos[:, None, None, None]
        spent = jnp.where(usable, jax.nn.softplus(score), 0.0)
        inside = jnp.dot(spent.reshape(-1, KBLK), upper, precision=lax.Precision.HIGHEST).reshape(
            spent.shape
        )
        totals = inside[..., 0]
        weight = jnp.where(usable, jnp.exp(score - inside), 0.0).astype(jnp.bfloat16)
        pieces = jnp.einsum(
            "qhbk,bkhd->qhbd", weight, value_block, preferred_element_type=jnp.float32
        )
        block_running = jnp.cumsum(totals, axis=-1)
        step_total = block_running[..., -1]
        beyond = step_total[..., None] - block_running
        factor = jnp.exp(-(behind[..., None] + beyond))
        summed = summed + jnp.sum(pieces * factor[..., None], axis=2)
        return (summed, behind + step_total)

    initial = (
        jnp.zeros((shard_len, heads_here, HEAD_DIM), jnp.float32),
        jnp.zeros((shard_len, heads_here), jnp.float32),
    )
    summed, _ = lax.fori_loop(0, visits, visit, initial)
    return summed.reshape(shard_len, heads_here * HEAD_DIM).astype(jnp.bfloat16)


def local(
    query_rows,
    key_rows,
    value_rows,
    residual,
    output_weight,
    first_gain,
    first_bias,
    expert_ids,
    expert_share,
    gate_weight,
    up_weight,
    down_weight,
    shared_gate,
    shared_up,
    shared_down,
    second_gain,
    second_bias,
):
    seq_index = lax.axis_index("sp")
    key_all, value_all = (
        lax.all_gather(key_rows, "sp", axis=0, tiled=True),
        lax.all_gather(value_rows, "sp", axis=0, tiled=True),
    )
    attended = stick_local(query_rows, key_all, value_all, seq_index)
    tokens_here = residual.shape[0]
    width = residual.shape[1]
    by_token = lax.all_to_all(attended, "tp", split_axis=0, concat_axis=1, tiled=True)
    mixed = jnp.dot(
        by_token,
        lax.all_gather(output_weight, "tp", axis=0, tiled=True),
        preferred_element_type=jnp.float32,
    )
    normed = layer_norm(residual.astype(jnp.float32) + mixed, first_gain, first_bias).astype(
        jnp.bfloat16
    )
    top_count = expert_ids.shape[1]
    pair_count = tokens_here * top_count
    experts = lax.axis_size("sp") * lax.axis_size("tp")
    capacity = max(2, 3 * pair_count // (2 * experts))
    flat_ids = expert_ids.reshape(pair_count)
    one_hot = (flat_ids[:, None] == jnp.arange(experts, dtype=jnp.int32)[None, :]).astype(
        jnp.bfloat16
    )
    earlier_mask = (jnp.arange(pair_count)[:, None] > jnp.arange(pair_count)[None, :]).astype(
        jnp.bfloat16
    )
    before = jnp.dot(earlier_mask, one_hot, preferred_element_type=jnp.float32)
    ranked = jnp.sum(before * one_hot, axis=1).astype(jnp.int32)
    slot_ids = flat_ids * capacity + ranked
    selector = jnp.any(
        slot_ids.reshape(tokens_here, top_count)[None, :, :]
        == jnp.arange(experts * capacity, dtype=jnp.int32)[:, None, None],
        axis=2,
    )
    outgoing = jnp.dot(selector.astype(jnp.bfloat16), normed, preferred_element_type=jnp.float32)
    outgoing = outgoing.astype(jnp.bfloat16).reshape(experts, capacity, width)
    slot_rows = lax.all_to_all(outgoing, ("sp", "tp"), split_axis=0, concat_axis=0, tiled=True)
    flat_rows = slot_rows.reshape(-1, width)
    gate_act = jnp.dot(flat_rows, gate_weight[0], preferred_element_type=jnp.float32)
    up_act = jnp.dot(flat_rows, up_weight[0], preferred_element_type=jnp.float32)
    hidden = (jax.nn.silu(gate_act) * up_act).astype(jnp.bfloat16)
    produced = jnp.dot(hidden, down_weight[0], preferred_element_type=jnp.float32).astype(
        jnp.bfloat16
    )
    results = produced.reshape(slot_rows.shape)
    returned = lax.all_to_all(results, ("sp", "tp"), split_axis=0, concat_axis=0, tiled=True)
    flat_back = returned.reshape(experts * capacity, width)
    picked = jnp.take(flat_back, slot_ids, axis=0).reshape(tokens_here, top_count, width)
    routed = jnp.sum(picked.astype(jnp.float32) * expert_share[:, :, None], axis=1)
    gate_act = jnp.dot(normed, shared_gate, preferred_element_type=jnp.float32)
    up_act = jnp.dot(normed, shared_up, preferred_element_type=jnp.float32)
    shared_hidden = (jax.nn.silu(gate_act) * up_act).astype(jnp.bfloat16)
    shared_out = jnp.dot(shared_hidden, shared_down, preferred_element_type=jnp.float32)
    final = layer_norm(normed.astype(jnp.float32) + routed + shared_out, second_gain, second_bias)
    return final.astype(jnp.bfloat16)


def solution(mesh):
    return jax.shard_map(
        local,
        mesh=mesh,
        in_specs=(
            P(("grp", "sp"), "tp"),
            P(("grp", "sp"), "tp"),
            P(("grp", "sp"), "tp"),
            P(("grp", "sp", "tp"), None),
            P("tp", None),
            P(),
            P(),
            P(("grp", "sp", "tp"), None),
            P(("grp", "sp", "tp"), None),
            P(("sp", "tp"), None, None),
            P(("sp", "tp"), None, None),
            P(("sp", "tp"), None, None),
            P(),
            P(),
            P(),
            P(),
            P(),
        ),
        out_specs=P(("grp", "sp", "tp"), None),
        check_vma=False,
    )
```

profile of v0, /device:TPU:11, one launch (start us, length us, event | category | flops | bytes accessed | tf_op | source)
XLA Modules:
  0.0 287.9 jit_solution(279792652444029237)
XLA Ops:
  6.5 0.7 all-gather.2.cloned.1.call-update
  7.3 13.9 %all_gather.10 = bf16[2048,128]{1,0:T(8,128)(2,1)} all-gather(bf16[512,128]{1,0:T(8,128)(2,1)} %param.20), channel_id=1, replica_groups=mesh['grp'=2,'sp'=4,'tp'=4] {'sp'}, dimensions={0}, use_global_device_ids=true | all-gather | bytes 655360 | tf_op jit(solution)/shard_map/all_gather | solution.py:93
  21.2 13.1 %all_gather.9 = bf16[2048,128]{1,0:T(8,128)(2,1)S(1)} all-gather(bf16[512,128]{1,0:T(8,128)(2,1)} %param.21), channel_id=1, replica_groups=mesh['grp'=2,'sp'=4,'tp'=4] {'sp'}, dimensions={0}, use_global_device_ids=true | all-gather | bytes 655360 | tf_op jit(solution)/shard_map/all_gather | solution.py:94
  34.3 22.5 %while.15 = (s32[]{:T(128)}, f32[512,1,128]{0,2,1:T(8,128)S(1)}, f32[512,1]{0,1:T(1,128)S(1)}, s32[]{:T(128)}, s32[]{:T(128)}, /*index=5*/bf16[2048,128]{1,0:T(8...) while((s32[]{:T(128)}, f32[512,1,128]{0,2,1:T(8,128)S(1)}, ...), condition=%wide.region_3.4_spmd.clone, body=%wide.region_0.3_spmd.clone.sunk | while | flops 1081683968 | bytes 25510100 | solution.py:68
  34.4 2.7 convolution_multiply_fusion.5
  37.1 2.9 %copy.83 = f32[512,1,1024]{2,0,1:T(8,128)} copy(f32[512,1,1024]{0,2,1:T(8,128)} %bitcast.106) | data formatting | bytes 4194304 | tf_op jit(solution)/shard_map/while/body/mul | solution.py:43
  40.0 2.7 reshape.289
  43.0 5.3 %fusion.90 = f32[4096,128]{1,0:T(8,128)} fusion(f32[4096,128]{1,0:T(8,128)} %reshape.289, s32[4096]{0:T(1024)S(1)} %lt.128, s32[8,128]{1,0:T(8,128)S(1)} %add_add_fusion.2), kind=kOutput, calls=%fused_computation.5.clone.1 | convolution fusion | flops 809533440 | bytes 4214784 | tf_op jit(solution)/shard_map/while/body/dot_general | solution.py:49
  48.3 2.2 copy.84
  50.6 2.9 %copy.82 = f32[512,8,128]{2,0,1:T(8,128)} copy(f32[512,8,128]{0,2,1:T(8,128)} %bitcast.107) | data formatting | bytes 4194304 | tf_op jit(solution)/shard_map/while/body/reshape | solution.py:46
  53.5 3.2 %fusion.92 = f32[512,128]{0,1:T(8,128)S(1)} fusion(bf16[8,128,128]{2,1,0:T(8,128)(2,1)S(1)} %bitcast.110, f32[512,8,128]{2,0,1:T(8,128)} %copy.82, f32[512,8,128]{2,1,0:T(8,128)} %bitcast.109, f32[512,8]{0,1:T(8,128)S(1)} %fusion.91, s32[8,128]{1,0:T(8,128)S(1)} %add_add_fusion.2, s32[512]{0:T(512)S(1)} %iota_add_fusion.2), kind=kOutput, calls=%fused_computation.7.clone.1 | convolution fusion | flops 137297920 | bytes 4741120 | tf_op jit(solution)/shard_map/while/body/qhbk,bkhd->qhbd/dot_general | solution.py:54
  56.8 0.8 copy.60
  57.6 8.7 %all-to-all-start = ((bf16[4,128,128]{2,1,0:T(8,128)(2,1)}), bf16[4,128,128]{2,1,0:T(8,128)(2,1)S(1)}, u32[]{:S(2)}, u32[]{:S(2)}) async-start(bf16[4,128,128]{2,1,0:T(8,128)(2,1)} %bitcast.1), calls=%async_computation | async-start | bytes 262144 | tf_op jit(solution)/shard_map/all_to_all | solution.py:99
  66.5 0.3 fusion.36
  67.2 1.8 all-to-all-done
  69.3 2.2 fusion.60
  71.5 0.3 multiply_reduce_fusion.2
  71.8 0.2 add_convert_fusion.1
  72.0 1.0 convolution_convert_fusion.1
  73.0 98.7 %all_to_all.26 = bf16[16,48,2048]{2,1,0:T(8,128)(2,1)S(1)} all-to-all(bf16[16,48,2048]{2,1,0:T(8,128)(2,1)S(1)} %bitcast.111), channel_id=1, replica_groups=mesh['grp'=2,'sp'=4,'tp'=4] {'sp','tp'}, dimensions={0} | all-to-all | bytes 6291456 | tf_op jit(solution)/shard_map/all_to_all | solution.py:129
  171.8 1.7 copy-done.3
  173.5 1.9 fusion.40
  175.3 7.7 %convolution_convert_fusion = bf16[768,2048]{1,0:T(8,128)(2,1)} fusion(bf16[768,2048]{1,0:T(8,128)(2,1)} %bitcast.115, bf16[1,256,2048]{2,1,0:T(8,128)(2,1)} %param.30, bf16[1,2048,256]{2,1,0:T(8,128)(2,1)} %param.29, f32[768,256]{1,0:T(8,128)} %fusion.40), kind=kOutput, calls=%fused_computation.43 | convolution fusion | flops 1613365248 | bytes 9175040 | tf_op jit(solution)/shard_map/dot_general | solution.py:134
  183.1 5.2 %all-to-all-start.2 = ((bf16[16,48,2048]{2,1,0:T(8,128)(2,1)}), bf16[16,48,2048]{2,1,0:T(8,128)(2,1)}, u32[]{:S(2)}, u32[]{:S(2)}) async-start(bf16[16,48,2048]{2,1,0:T(8,128)(2,1)} %bitcast.113), calls=%async_computation.2 | async-start | bytes 6291456 | tf_op jit(solution)/shard_map/all_to_all | solution.py:138
  188.8 2.0 fusion.62
  190.9 67.4 %all-to-all-done.2 = bf16[16,48,2048]{2,1,0:T(8,128)(2,1)} async-done(((bf16[16,48,2048]{2,1,0:T(8,128)(2,1)}), bf16[16,48,2048]{2,1,0:T(8,128)(2,1)}, u32[]{:S(2)}, u32[]{:S(2)}) %all-to-all-start.2) | async-done | bytes 3145760 | tf_op jit(solution)/shard_map/all_to_all | solution.py:138
  258.3 7.6 %gather_fusion = bf16[512,2048]{1,0:T(8,128)(2,1)} fusion(bf16[768,2048]{1,0:T(8,128)(2,1)} %bitcast.10, s32[1024]{0:T(1024)S(1)} %pad_clamp_fusion), kind=kCustom, calls=%fused_computation | custom fusion | bytes 4196352 | tf_op jit(solution)/shard_map/jit(_take)/gather | solution.py:140
  265.9 4.1 %gather.7 = bf16[128,4,2048]{2,1,0:T(4,128)(2,1)} reshape(bf16[512,2048]{1,0:T(8,128)(2,1)} %gather_fusion) | data formatting | bytes 4194304 | tf_op jit(solution)/shard_map/jit(_take)/gather | solution.py:140
  270.0 6.6 %multiply_reduce_fusion = f32[128,2048]{1,0:T(8,128)} fusion(f32[128,4]{1,0:T(8,128)S(1)} %copy.66, bf16[128,4,2048]{2,1,0:T(4,128)(2,1)} %gather.7, pred[128,4]{1,0:T(8,128)(4,1)S(1)} %copy.64), kind=kLoop, calls=%fused_computation.42 | loop fusion | flops 3932160 | bytes 3148288 | tf_op jit(solution)/shard_map/reduce_sum | solution.py:141
  276.6 3.1 %fusion.61 = (f32[128]{0:T(128)S(1)}, f32[128,2048]{1,0:T(8,128)S(1)}) fusion(bf16[512,2048]{1,0:T(8,128)(2,1)S(1)} %copy-done, bf16[128,2048]{1,0:T(8,128)(2,1)} %copy-done.1, bf16[2048,512]{1,0:T(8,128)(2,1)} %param.32, f32[128,512]{1,0:T(8,128)S(1)} %fusion.62, f32[128,2048]{1,0:T(8,128)} %multiply_reduce_fusion), kind=kOutput, calls=%fused_computation.92 | convolution fusion | flops 538312576 | bytes 7078400 | tf_op jit(solution)/shard_map/dot_general | solution.py:145
  279.7 0.3 multiply_reduce_fusion.1
  280.0 1.0 add_convert_fusion
  (54 shorter events, 1.8 us)
Async XLA Ops:
  6.5 270.0 %copy-start = (bf16[512,2048]{1,0:T(8,128)(2,1)S(1)}, bf16[512,2048]{1,0:T(8,128)(2,1)}, u32[]{:S(2)}) copy-start(bf16[512,2048]{1,0:T(8,128)(2,1)} %param.33) | copy-start | bytes 6291460
  6.5 27.8 %copy-start.2 = (bf16[512,128]{1,0:T(8,128)(2,1)S(1)}, bf16[512,128]{1,0:T(8,128)(2,1)}, u32[]{:S(2)}) copy-start(bf16[512,128]{1,0:T(8,128)(2,1)} %param.19) | copy-start | bytes 393220
  6.5 62.7 %all-gather.2.cloned.1.call-start = ((), (), s32[]{:S(2)}) async-start(), calls=%async_computation.3 | async-start | bytes 2621440 | tf_op jit(solution)/shard_map/all_gather | solution.py:102
  34.3 32.0 %copy-start.4 = (s32[128,4]{0,1:T(4,128)S(1)}, s32[128,4]{0,1:T(4,128)}, u32[]{:S(2)}) copy-start(s32[128,4]{0,1:T(4,128)} %param.26) | copy-start | bytes 6148
  57.6 11.5 %all-to-all-start = ((bf16[4,128,128]{2,1,0:T(8,128)(2,1)}), bf16[4,128,128]{2,1,0:T(8,128)(2,1)S(1)}, u32[]{:S(2)}, u32[]{:S(2)}) async-start(bf16[4,128,128]{2,1,0:T(8,128)(2,1)} %bitcast.1), calls=%async_computation | async-start | bytes 262144 | tf_op jit(solution)/shard_map/all_to_all | solution.py:99
  69.2 2.5 copy-start.5
  69.2 2.5 copy-start.6
  72.0 116.8 %copy-start.1 = (bf16[128,2048]{1,0:T(8,128)(2,1)}, bf16[128,2048]{1,0:T(8,128)(2,1)S(1)}, u32[]{:S(2)}) copy-start(bf16[128,2048]{1,0:T(8,128)(2,1)S(1)} %add_convert_fusion.1) | copy-start | bytes 1572868
  73.0 100.4 %copy-start.10 = (bf16[1,2048,256]{2,1,0:T(8,128)(2,1)S(1)}, bf16[1,2048,256]{2,1,0:T(8,128)(2,1)}, u32[]{:S(2)}) copy-start(bf16[1,2048,256]{2,1,0:T(8,128)(2,1)} %param.28) | copy-start | bytes 3145732
  171.8 1.7 copy-start.3
  183.0 5.6 %copy-start.9 = (f32[128,4]{0,1:T(4,128)S(1)}, f32[128,4]{0,1:T(4,128)}, u32[]{:S(2)}) copy-start(f32[128,4]{0,1:T(4,128)} %param.27) | copy-start | bytes 6148
  183.1 75.2 %all-to-all-start.2 = ((bf16[16,48,2048]{2,1,0:T(8,128)(2,1)}), bf16[16,48,2048]{2,1,0:T(8,128)(2,1)}, u32[]{:S(2)}, u32[]{:S(2)}) async-start(bf16[16,48,2048]{2,1,0:T(8,128)(2,1)} %bitcast.113), calls=%async_computation.2 | async-start | bytes 6291456 | tf_op jit(solution)/shard_map/all_to_all | solution.py:138
  276.6 3.4 %copy-start.7 = (f32[2048]{0:T(1024)S(1)}, f32[2048]{0:T(1024)}, u32[]{:S(2)}) copy-start(f32[2048]{0:T(1024)} %param.35) | copy-start | bytes 24580
  276.6 3.4 %copy-start.8 = (f32[2048]{0:T(1024)S(1)}, f32[2048]{0:T(1024)}, u32[]{:S(2)}) copy-start(f32[2048]{0:T(1024)} %param.34) | copy-start | bytes 24580
Sparse Core Ops, SparseCore 0:
  8.9 23.1 all-gather.1
where the time goes:
time: 289 us; the launch traced here: 288 us
  blocking collectives  126 us (44%)
  waiting for transfers between devices  70 us (24%)
  matrix products  29.4 us (10%)
  local copies, waits for them, and re-layouts  26.3 us (9%)
  starting transfers between devices  13.9 us (5%)
  between operations  13.6 us (5%)
  other arithmetic  8.8 us (3%)
    all_to_all x1, blocking collectives, local(): lax.all_to_all(outgoing, ('sp', 'tp'), split_axis=0, concat_axis=0, tiled...  98.7 us
    all_to_all x1, waiting for transfers between devices, local(): lax.all_to_all(results, ('sp', 'tp'), split_axis=0, concat_axis=0, tiled=...  67.4 us
    all_gather x1, blocking collectives, local(): lax.all_gather(key_rows, 'sp', axis=0, tiled=True)  13.9 us
    all_gather x1, blocking collectives, local(): lax.all_gather(value_rows, 'sp', axis=0, tiled=True)  13.1 us
    gather x2, local copies, waits for them, and re-layouts, local(): jnp.take(flat_back, slot_ids, axis=0).reshape(tokens_here, top_count, width)  11.7 us
    all_to_all x1, starting transfers between devices, local(): lax.all_to_all(attended, 'tp', split_axis=0, concat_axis=1, tiled=True)  8.71 us
    dot_general x1, matrix products, local(): jnp.dot(hidden, down_weight[0], preferred_element_type=jnp.float32)  7.72 us
    reduce_sum x1, other arithmetic, local(): jnp.sum(picked.astype(jnp.float32) * expert_share[:, :, None], axis=1)  6.57 us
  transfers between devices with their start and end apart: 3, of which 2 were waited for; matrix products, arithmetic and copies ran while one was open for 9% of the time, Pallas kernels for 0%

commit v1 on v0

--- a/solution.py
+++ b/solution.py
@@ -67,6 +67,70 @@
     )
     summed, _ = lax.fori_loop(0, visits, visit, initial)
     return summed.reshape(shard_len, heads_here * HEAD_DIM).astype(jnp.bfloat16)
+
+
+def slot_capacity(pair_count, experts):
+    return max(2, 3 * pair_count // (2 * experts))
+
+
+def routed_slots(normed, expert_ids, expert_share, gate_weight, up_weight, down_weight):
+    tokens_here, width = normed.shape
+    top_count = expert_ids.shape[1]
+    pair_count = tokens_here * top_count
+    experts = lax.axis_size("sp") * lax.axis_size("tp")
+    capacity = slot_capacity(pair_count, experts)
+    flat_ids = expert_ids.reshape(pair_count)
+    one_hot = (flat_ids[:, None] == jnp.arange(experts, dtype=jnp.int32)[None, :]).astype(
+        jnp.bfloat16
+    )
+    earlier_mask = (jnp.arange(pair_count)[:, None] > jnp.arange(pair_count)[None, :]).astype(
+        jnp.bfloat16
+    )
+    before = jnp.dot(earlier_mask, one_hot, preferred_element_type=jnp.float32)
+    ranked = jnp.sum(before * one_hot, axis=1).astype(jnp.int32)
+    slot_ids = flat_ids * capacity + ranked
+    selector = jnp.any(
+        slot_ids.reshape(tokens_here, top_count)[None, :, :]
+        == jnp.arange(experts * capacity, dtype=jnp.int32)[:, None, None],
+        axis=2,
+    )
+    outgoing = jnp.dot(selector.astype(jnp.bfloat16), normed, preferred_element_type=jnp.float32)
+    outgoing = outgoing.astype(jnp.bfloat16).reshape(experts, capacity, width)
+    slot_rows = lax.all_to_all(outgoing, ("sp", "tp"), split_axis=0, concat_axis=0, tiled=True)
+    flat_rows = slot_rows.reshape(-1, width)
+    gate_act = jnp.dot(flat_rows, gate_weight[0], preferred_element_type=jnp.float32)
+    up_act = jnp.dot(flat_rows, up_weight[0], preferred_element_type=jnp.float32)
+    hidden = (jax.nn.silu(gate_act) * up_act).astype(jnp.bfloat16)
+    produced = jnp.dot(hidden, down_weight[0], preferred_element_type=jnp.float32).astype(
+        jnp.bfloat16
+    )
+    results = produced.reshape(slot_rows.shape)
+    returned = lax.all_to_all(results, ("sp", "tp"), split_axis=0, concat_axis=0, tiled=True)
+    flat_back = returned.reshape(experts * capacity, width)
+    picked = jnp.take(flat_back, slot_ids, axis=0).reshape(tokens_here, top_count, width)
+    routed = jnp.sum(picked.astype(jnp.float32) * expert_share[:, :, None], axis=1)
+    return routed
+
+
+def expert_dense(rows, ids_all, share_all, expert, gate_mat, up_mat, down_mat):
+    weight = jnp.sum(jnp.where(ids_all == expert, share_all, 0.0), axis=1, keepdims=True)
+    gate_act = jnp.dot(rows, gate_mat, preferred_element_type=jnp.float32)
+    up_act = jnp.dot(rows, up_mat, preferred_element_type=jnp.float32)
+    hidden = (jax.nn.silu(gate_act) * up_act).astype(jnp.bfloat16)
+    produced = jnp.dot(hidden, down_mat, preferred_element_type=jnp.float32)
+    return (produced * weight).astype(jnp.bfloat16)
+
+
+def routed_dense(normed, expert_ids, expert_share, gate_weight, up_weight, down_weight):
+    axes = ("sp", "tp")
+    expert = lax.axis_index("sp") * lax.axis_size("tp") + lax.axis_index("tp")
+    rows = lax.all_gather(normed, axes, axis=0, tiled=True)
+    ids_all = lax.all_gather(expert_ids, axes, axis=0, tiled=True)
+    share_all = lax.all_gather(expert_share, axes, axis=0, tiled=True)
+    parts = expert_dense(
+        rows, ids_all, share_all, expert, gate_weight[0], up_weight[0], down_weight[0]
+    )
+    return lax.psum_scatter(parts, axes, scatter_dimension=0, tiled=True).astype(jnp.float32)
 
 
 def local(
@@ -95,7 +159,6 @@
     )
     attended = stick_local(query_rows, key_all, value_all, seq_index)
     tokens_here = residual.shape[0]
-    width = residual.shape[1]
     by_token = lax.all_to_all(attended, "tp", split_axis=0, concat_axis=1, tiled=True)
     mixed = jnp.dot(
         by_token,
@@ -105,40 +168,10 @@
     normed = layer_norm(residual.astype(jnp.float32) + mixed, first_gain, first_bias).astype(
         jnp.bfloat16
     )
-    top_count = expert_ids.shape[1]
-    pair_count = tokens_here * top_count
     experts = lax.axis_size("sp") * lax.axis_size("tp")
-    capacity = max(2, 3 * pair_count // (2 * experts))
-    flat_ids = expert_ids.reshape(pair_count)
-    one_hot = (flat_ids[:, None] == jnp.arange(experts, dtype=jnp.int32)[None, :]).astype(
-        jnp.bfloat16
-    )
-    earlier_mask = (jnp.arange(pair_count)[:, None] > jnp.arange(pair_count)[None, :]).astype(
-        jnp.bfloat16
-    )
-    before = jnp.dot(earlier_mask, one_hot, preferred_element_type=jnp.float32)
-    ranked = jnp.sum(before * one_hot, axis=1).astype(jnp.int32)
-    slot_ids = flat_ids * capacity + ranked
-    selector = jnp.any(
-        slot_ids.reshape(tokens_here, top_count)[None, :, :]
-        == jnp.arange(experts * capacity, dtype=jnp.int32)[:, None, None],
-        axis=2,
-    )
-    outgoing = jnp.dot(selector.astype(jnp.bfloat16), normed, preferred_element_type=jnp.float32)
-    outgoing = outgoing.astype(jnp.bfloat16).reshape(experts, capacity, width)
-    slot_rows = lax.all_to_all(outgoing, ("sp", "tp"), split_axis=0, concat_axis=0, tiled=True)
-    flat_rows = slot_rows.reshape(-1, width)
-    gate_act = jnp.dot(flat_rows, gate_weight[0], preferred_element_type=jnp.float32)
-    up_act = jnp.dot(flat_rows, up_weight[0], preferred_element_type=jnp.float32)
-    hidden = (jax.nn.silu(gate_act) * up_act).astype(jnp.bfloat16)
-    produced = jnp.dot(hidden, down_weight[0], preferred_element_type=jnp.float32).astype(
-        jnp.bfloat16
-    )
-    results = produced.reshape(slot_rows.shape)
-    returned = lax.all_to_all(results, ("sp", "tp"), split_axis=0, concat_axis=0, tiled=True)
-    flat_back = returned.reshape(experts * capacity, width)
-    picked = jnp.take(flat_back, slot_ids, axis=0).reshape(tokens_here, top_count, width)
-    routed = jnp.sum(picked.astype(jnp.float32) * expert_share[:, :, None], axis=1)
+    slots = experts * slot_capacity(tokens_here * expert_ids.shape[1], experts)
+    routed_fn = routed_dense if tokens_here * experts <= 4 * slots else routed_slots
+    routed = routed_fn(normed, expert_ids, expert_share, gate_weight, up_weight, down_weight)
     gate_act = jnp.dot(normed, shared_gate, preferred_element_type=jnp.float32)
     up_act = jnp.dot(normed, shared_up, preferred_element_type=jnp.float32)
     shared_hidden = (jax.nn.silu(gate_act) * up_act).astype(jnp.bfloat16)

time: 289 us -> 307 us (1.062)
  waiting for transfers between devices: 70 us -> 138 us
  blocking collectives: 126 us -> 98.8 us
  local copies, waits for them, and re-layouts: 26.3 us -> 12.4 us
  starting transfers between devices: 13.9 us -> 0.08 us
  matrix products: 29.4 us -> 39.3 us
  other arithmetic: 8.8 us -> 2.79 us
    reduce_scatter x0 -> x1, waiting for transfers between devices: none -> 99.6 us  [routed_dense(): lax.psum_scatter(parts, axes, scatter_dimension=0, tiled=True)]
    all_to_all x1, blocking collectives: 98.7 us -> 12 us  [local(): lax.all_to_all(attended, 'tp', split_axis=0, concat_axis=1, tiled=True)]
    all_to_all x2 -> x0, waiting for transfers between devices: 69.3 us -> none  [the longest x1 67.4 us: local(): lax.all_to_all(results, ('sp', 'tp'), split_axis=0, concat_axis=0, tiled=...]
    all_gather x0 -> x2, blocking collectives: none -> 60.2 us  [the longest x1 39.4 us: routed_dense(): ids_all = lax.all_gather(expert_ids, axes, axis=0, tiled=True)]
    all_gather x0 -> x1, waiting for transfers between devices: none -> 37.2 us  [routed_dense(): rows = lax.all_gather(normed, axes, axis=0, tiled=True)]
    all_to_all x2 -> x0, starting transfers between devices: 13.9 us -> none  [the longest x1 8.71 us: local(): lax.all_to_all(attended, 'tp', split_axis=0, concat_axis=1, tiled=True)]
    gather x2 -> x0, local copies, waits for them, and re-layouts: 11.7 us -> none  [local(): jnp.take(flat_back, slot_ids, axis=0).reshape(tokens_here, top_count, width)]
    dot_general x4 -> x2, matrix products: 10.8 us -> 20.9 us  [the longest x1 13.8 us: expert_dense(): produced = jnp.dot(hidden, down_mat, preferred_element_type=jnp.float32)]
  transfers between devices with their start and end apart: 3 -> 3, of which waited for: 2 -> 2; matrix products, arithmetic and copies ran while one was open for 9% -> 8% of each run, Pallas kernels for 0% -> 0%
where the time goes in v1:
time: 307 us; the launch traced here: 304 us
  waiting for transfers between devices  138 us (45%)
  blocking collectives  98.8 us (32%)
  matrix products  39.3 us (13%)
  between operations  13.3 us (4%)
  local copies, waits for them, and re-layouts  12.4 us (4%)
    reduce_scatter x1, waiting for transfers between devices, routed_dense(): lax.psum_scatter(parts, axes, scatter_dimension=0, tiled=True)  99.6 us
    all_gather x1, blocking collectives, routed_dense(): ids_all = lax.all_gather(expert_ids, axes, axis=0, tiled=True)  39.4 us
    all_gather x1, waiting for transfers between devices, routed_dense(): rows = lax.all_gather(normed, axes, axis=0, tiled=True)  37.2 us
    all_gather x1, blocking collectives, routed_dense(): share_all = lax.all_gather(expert_share, axes, axis=0, tiled=True)  20.8 us
    dot_general x1, matrix products, expert_dense(): produced = jnp.dot(hidden, down_mat, preferred_element_type=jnp.float32)  13.8 us
    all_gather x1, blocking collectives, local(): lax.all_gather(key_rows, 'sp', axis=0, tiled=True)  13.3 us
    all_gather x1, blocking collectives, local(): lax.all_gather(value_rows, 'sp', axis=0, tiled=True)  13.3 us
    all_to_all x1, blocking collectives, local(): lax.all_to_all(attended, 'tp', split_axis=0, concat_axis=1, tiled=True)  12 us
  transfers between devices with their start and end apart: 3, of which 2 were waited for; matrix products, arithmetic and copies ran while one was open for 8% of the time, Pallas kernels for 0%

profile of v1, /device:TPU:11, one launch (start us, length us, event | category | flops | bytes accessed | tf_op | source)
XLA Modules:
  0.0 304.4 jit_solution(2174168436149483998)
XLA Ops:
  6.5 0.7 all-gather.3.cloned.1.call-update
  7.3 13.3 %all_gather.18 = bf16[2048,128]{1,0:T(8,128)(2,1)S(1)} all-gather(bf16[512,128]{1,0:T(8,128)(2,1)} %param.21), channel_id=1, replica_groups=mesh['grp'=2,'sp'=4,'tp'=4] {'sp'}, dimensions={0}, use_global_device_ids=true | all-gather | bytes 655360 | tf_op jit(solution)/shard_map/all_gather | solution.py:158
  20.6 13.3 %all_gather.19 = bf16[2048,128]{1,0:T(8,128)(2,1)} all-gather(bf16[512,128]{1,0:T(8,128)(2,1)} %param.20), channel_id=1, replica_groups=mesh['grp'=2,'sp'=4,'tp'=4] {'sp'}, dimensions={0}, use_global_device_ids=true | all-gather | bytes 655360 | tf_op jit(solution)/shard_map/all_gather | solution.py:157
  34.0 22.5 %while.15 = (s32[]{:T(128)}, f32[512,1,128]{0,2,1:T(8,128)S(1)}, f32[512,1]{0,1:T(1,128)S(1)}, s32[]{:T(128)}, s32[]{:T(128)}, /*index=5*/bf16[2048,128]{1,0:T(8...) while((s32[]{:T(128)}, f32[512,1,128]{0,2,1:T(8,128)S(1)}, ...), condition=%wide.region_3.4_spmd.clone, body=%wide.region_0.3_spmd.clone.sunk | while | flops 1081683968 | bytes 25510100 | solution.py:68
  34.0 2.7 convolution_multiply_fusion.4
  36.7 2.9 copy.51
  39.6 2.7 reshape.206
  42.4 0.1 lt.95
  42.5 0.2 lt.96
  42.7 5.3 %fusion.77 = f32[4096,128]{1,0:T(8,128)} fusion(f32[4096,128]{1,0:T(8,128)} %reshape.206, s32[4096]{0:T(1024)S(1)} %lt.96, s32[8,128]{1,0:T(8,128)S(1)} %add_add_fusion.2), kind=kOutput, calls=%fused_computation.4.clone.1 | convolution fusion | flops 809533440 | bytes 4214784 | tf_op jit(solution)/shard_map/while/body/dot_general | solution.py:49
  47.9 2.2 copy.52
  50.2 2.9 copy.50
  53.1 3.2 %fusion.79 = f32[512,128]{0,1:T(8,128)S(1)} fusion(bf16[8,128,128]{2,1,0:T(8,128)(2,1)S(1)} %bitcast.102, f32[512,8,128]{2,0,1:T(8,128)} %copy.50, f32[512,8,128]{2,1,0:T(8,128)} %bitcast.101, f32[512,8]{0,1:T(8,128)S(1)} %fusion.78, s32[8,128]{1,0:T(8,128)S(1)} %add_add_fusion.2, s32[512]{0:T(512)S(1)} %iota_add_fusion.2), kind=kOutput, calls=%fused_computation.6.clone.1 | convolution fusion | flops 137297920 | bytes 4741120 | tf_op jit(solution)/shard_map/while/body/qhbk,bkhd->qhbd/dot_general | solution.py:54
  56.4 0.1 bitcast_add_fusion.4
  56.5 0.1 copy.33
  56.6 12.0 %all_to_all.16 = bf16[4,128,128]{2,1,0:T(8,128)(2,1)S(1)} all-to-all(bf16[4,128,128]{2,1,0:T(8,128)(2,1)S(1)} %bitcast.106), channel_id=1, replica_groups=mesh['grp'=2,'sp'=4,'tp'=4] {'tp'}, dimensions={0} | all-to-all | bytes 262144 | tf_op jit(solution)/shard_map/all_to_all | solution.py:162
  68.6 0.1 copy.34
  68.8 2.2 fusion.49
  71.1 0.3 multiply_reduce_fusion.1
  71.3 1.0 add_convert_fusion.1
  72.4 0.0 reduce-scatter.2.cloned.1.call-start
  72.5 39.4 %all_gather.22 = s32[2048,4]{0,1:T(4,128)S(1)} all-gather(s32[128,4]{0,1:T(4,128)S(1)} %copy-done.7), channel_id=1, replica_groups=mesh['grp'=2,'sp'=4,'tp'=4] {'sp','tp'}, dimensions={0}, use_global_device_ids=true | all-gather | bytes 34816 | tf_op jit(solution)/shard_map/all_gather | solution.py:128
  111.9 20.8 %all_gather.23 = f32[2048,4]{0,1:T(4,128)S(1)} all-gather(f32[128,4]{0,1:T(4,128)S(1)} %copy-done.8), channel_id=1, replica_groups=mesh['grp'=2,'sp'=4,'tp'=4] {'sp','tp'}, dimensions={0}, use_global_device_ids=true | all-gather | bytes 34816 | tf_op jit(solution)/shard_map/all_gather | solution.py:129
  132.7 37.2 %all-gather.5.cloned.1.call-done = bf16[2048,2048]{1,0:T(8,128)(2,1)} async-done(((bf16[128,2048]{1,0:T(8,128)(2,1)}), bf16[2048,2048]{1,0:T(8,128)(2,1)}) %all-gather.5.cloned.1.call-update) | async-done | bytes 8388624 | tf_op jit(solution)/shard_map/all_gather | solution.py:127
  169.9 7.1 %fusion.38 = f32[2048,256]{1,0:T(8,128)} fusion(bf16[2048,2048]{1,0:T(8,128)(2,1)} %all-gather.5.cloned.1.call-done, bf16[1,2048,256]{2,1,0:T(8,128)(2,1)S(1)} %copy-done.9), kind=kOutput, calls=%fused_computation.50 | convolution fusion | flops 2147483648 | bytes 11534336 | tf_op jit(solution)/shard_map/dot_general | solution.py:117
  177.0 13.8 %multiply_convert_fusion = bf16[2048,2048]{1,0:T(8,128)(2,1)} fusion(f32[2048]{0:T(1024)S(1)} %select_reduce_fusion, bf16[2048,2048]{1,0:T(8,128)(2,1)} %all-gather.5.cloned.1.call-done, f32[2048,256]{1,0:T(8,128)} %fusion.38, bf16[1,256,2048]{2,1,0:T(8,128)(2,1)} %param.30, bf16[1,2048,256]{2,1,0:T(8,128)(2,1)} %param.29), kind=kOutput, calls=%fused_computation.41 | convolution fusion | flops 4306501632 | bytes 20979712 | tf_op jit(solution)/shard_map/dot_general | solution.py:120
  190.9 1.0 copy-done.1
  191.9 2.0 fusion.51
  193.9 99.6 %reduce-scatter.2.cloned.1.call-done = bf16[128,2048]{1,0:T(8,128)(2,1)} async-done(((bf16[2048,2048]{1,0:T(8,128)(2,1)}), bf16[128,2048]{1,0:T(8,128)(2,1)}) %reduce-scatter.2.cloned.1.call-update) | async-done | bytes 524304 | tf_op jit(solution)/shard_map/reduce_scatter | solution.py:133
  293.6 2.9 fusion.50
  296.5 0.3 multiply_reduce_fusion
  296.8 1.0 add_convert_fusion
  (38 shorter events, 0.3 us)
Async XLA Ops:
  6.5 287.0 %copy-start = (bf16[512,2048]{1,0:T(8,128)(2,1)S(1)}, bf16[512,2048]{1,0:T(8,128)(2,1)}, u32[]{:S(2)}) copy-start(bf16[512,2048]{1,0:T(8,128)(2,1)} %param.33) | copy-start | bytes 6291460
  6.5 27.4 %copy-start.2 = (bf16[512,128]{1,0:T(8,128)(2,1)S(1)}, bf16[512,128]{1,0:T(8,128)(2,1)}, u32[]{:S(2)}) copy-start(bf16[512,128]{1,0:T(8,128)(2,1)} %param.19) | copy-start | bytes 393220
  6.5 62.2 %all-gather.3.cloned.1.call-start = ((), (), s32[]{:S(2)}) async-start(), calls=%async_computation.2 | async-start | bytes 2621440 | tf_op jit(solution)/shard_map/all_gather | solution.py:165
  7.3 162.7 %all-gather.5.cloned.1.call-start = ((), (), s32[]{:S(2)}) async-start(), calls=%async_computation.3 | async-start | bytes 8912896 | tf_op jit(solution)/shard_map/all_gather | solution.py:127
  68.8 2.6 copy-start.3
  68.8 2.6 copy-start.4
  71.0 1.5 copy-start.7
  71.0 40.9 %copy-start.8 = (f32[128,4]{0,1:T(4,128)S(1)}, f32[128,4]{0,1:T(4,128)}, u32[]{:S(2)}) copy-start(f32[128,4]{0,1:T(4,128)} %param.27) | copy-start | bytes 6148
  71.0 98.9 %copy-start.9 = (bf16[1,2048,256]{2,1,0:T(8,128)(2,1)S(1)}, bf16[1,2048,256]{2,1,0:T(8,128)(2,1)}, u32[]{:S(2)}) copy-start(bf16[1,2048,256]{2,1,0:T(8,128)(2,1)} %param.28) | copy-start | bytes 3145732
  72.4 221.2 %reduce-scatter.2.cloned.1.call-start = ((), (), s32[]{:S(2)}) async-start(), calls=%async_computation.4 | async-start | bytes 8912896 | tf_op jit(solution)/shard_map/reduce_scatter | solution.py:133
  190.8 1.0 copy-start.1
  193.9 102.9 %copy-start.5 = (f32[2048]{0:T(1024)S(1)}, f32[2048]{0:T(1024)}, u32[]{:S(2)}) copy-start(f32[2048]{0:T(1024)} %param.35) | copy-start | bytes 24580
  193.9 102.9 %copy-start.6 = (f32[2048]{0:T(1024)S(1)}, f32[2048]{0:T(1024)}, u32[]{:S(2)}) copy-start(f32[2048]{0:T(1024)} %param.34) | copy-start | bytes 24580
Sparse Core Ops, SparseCore 0:
  8.9 23.1 all-gather.2
  72.5 97.3 all-gather.4
  191.0 102.5 reduce-scatter.1

commit v2 on v0

--- a/solution.py
+++ b/solution.py
@@ -1,6 +1,10 @@
+import functools
+
 import jax
 import jax.numpy as jnp
 from jax import lax
+from jax.experimental import pallas as pl
+from jax.experimental.pallas import tpu as pltpu
 from jax.sharding import PartitionSpec as P
 
 HEAD_DIM = 128
@@ -67,6 +71,65 @@
     )
     summed, _ = lax.fori_loop(0, visits, visit, initial)
     return summed.reshape(shard_len, heads_here * HEAD_DIM).astype(jnp.bfloat16)
+
+
+def exchange_kernel(n_sp, n_tp, src, dst, send_sem, recv_sem, own_sem):
+    count = n_sp * n_tp
+    me = lax.axis_index("sp") * n_tp + lax.axis_index("tp")
+
+    def place(peer):
+        return {"sp": peer // n_tp, "tp": lax.rem(peer, n_tp)}
+
+    def copy(step, peer, landing):
+        return pltpu.make_async_remote_copy(
+            src_ref=src.at[peer],
+            dst_ref=dst.at[landing],
+            send_sem=send_sem.at[step],
+            recv_sem=recv_sem.at[step],
+            device_id=place(peer),
+            device_id_type=pl.DeviceIdType.MESH,
+        )
+
+    barrier = pltpu.get_barrier_semaphore()
+
+    @pl.loop(1, count)
+    def _(step):
+        peer = lax.rem(me + step, count)
+        pl.semaphore_signal(
+            barrier, inc=1, device_id=place(peer), device_id_type=pl.DeviceIdType.MESH
+        )
+
+    pl.semaphore_wait(barrier, count - 1)
+    own = pltpu.make_async_copy(src.at[me], dst.at[me], own_sem)
+    own.start()
+
+    @pl.loop(1, count)
+    def _(step):
+        copy(step, lax.rem(me + step, count), me).start()
+
+    own.wait()
+
+    @pl.loop(1, count)
+    def _(step):
+        copy(step, lax.rem(me + step, count), lax.rem(me + count - step, count)).wait()
+
+
+def exchange(blocks, collective_id):
+    n_sp, n_tp = lax.axis_size("sp"), lax.axis_size("tp")
+    return pl.pallas_call(
+        functools.partial(exchange_kernel, n_sp, n_tp),
+        out_shape=jax.ShapeDtypeStruct(blocks.shape, blocks.dtype),
+        in_specs=[pl.BlockSpec(memory_space=pl.ANY)],
+        out_specs=pl.BlockSpec(memory_space=pl.ANY),
+        scratch_shapes=[
+            pltpu.SemaphoreType.DMA((n_sp * n_tp,)),
+            pltpu.SemaphoreType.DMA((n_sp * n_tp,)),
+            pltpu.SemaphoreType.DMA,
+        ],
+        compiler_params=pltpu.CompilerParams(
+            collective_id=collective_id, has_side_effects=True
+        ),
+    )(blocks)
 
 
 def local(
@@ -126,7 +189,7 @@
     )
     outgoing = jnp.dot(selector.astype(jnp.bfloat16), normed, preferred_element_type=jnp.float32)
     outgoing = outgoing.astype(jnp.bfloat16).reshape(experts, capacity, width)
-    slot_rows = lax.all_to_all(outgoing, ("sp", "tp"), split_axis=0, concat_axis=0, tiled=True)
+    slot_rows = exchange(outgoing, 1)
     flat_rows = slot_rows.reshape(-1, width)
     gate_act = jnp.dot(flat_rows, gate_weight[0], preferred_element_type=jnp.float32)
     up_act = jnp.dot(flat_rows, up_weight[0], preferred_element_type=jnp.float32)
@@ -135,10 +198,16 @@
         jnp.bfloat16
     )
     results = produced.reshape(slot_rows.shape)
-    returned = lax.all_to_all(results, ("sp", "tp"), split_axis=0, concat_axis=0, tiled=True)
+    returned = exchange(results, 2)
     flat_back = returned.reshape(experts * capacity, width)
-    picked = jnp.take(flat_back, slot_ids, axis=0).reshape(tokens_here, top_count, width)
-    routed = jnp.sum(picked.astype(jnp.float32) * expert_share[:, :, None], axis=1)
+    placed = slot_ids.reshape(tokens_here, top_count)[:, :, None] == jnp.arange(
+        experts * capacity, dtype=jnp.int32
+    )
+    shares = jnp.sum(jnp.where(placed, expert_share[:, :, None], 0.0), axis=1)
+    upper_part = lax.reduce_precision(shares, 8, 7)
+    both = jnp.concatenate([upper_part, shares - upper_part], axis=0).astype(jnp.bfloat16)
+    both_out = jnp.dot(both, flat_back, preferred_element_type=jnp.float32)
+    routed = both_out[:tokens_here] + both_out[tokens_here:]
     gate_act = jnp.dot(normed, shared_gate, preferred_element_type=jnp.float32)
     up_act = jnp.dot(normed, shared_up, preferred_element_type=jnp.float32)
     shared_hidden = (jax.nn.silu(gate_act) * up_act).astype(jnp.bfloat16)

time: 289 us -> 273 us (0.945)
  Pallas kernels: 0 us -> 168 us
  blocking collectives: 126 us -> 27 us
  waiting for transfers between devices: 70 us -> 1.21 us
  local copies, waits for them, and re-layouts: 26.3 us -> 12.8 us
  matrix products: 29.4 us -> 37.8 us
  other arithmetic: 8.8 us -> 3.12 us
  starting transfers between devices: 13.9 us -> 8.72 us
    pallas_call x0 -> x2, Pallas kernels: none -> 168 us  [exchange(): pl.pallas_call(functools.partial(exchange_kernel, n_sp, n_tp), out_shape=...]
    all_to_all x1 -> x0, blocking collectives: 98.7 us -> none  [local(): lax.all_to_all(outgoing, ('sp', 'tp'), split_axis=0, concat_axis=0, tiled...]
    all_to_all x1 -> x0, waiting for transfers between devices: 67.4 us -> none  [local(): lax.all_to_all(results, ('sp', 'tp'), split_axis=0, concat_axis=0, tiled=...]
    gather x2 -> x0, local copies, waits for them, and re-layouts: 11.7 us -> none  [local(): jnp.take(flat_back, slot_ids, axis=0).reshape(tokens_here, top_count, width)]
    reduce_sum x1, other arithmetic: 6.57 us -> 0.24 us  [local(): shares = jnp.sum(jnp.where(placed, expert_share[:, :, None], 0.0), axis=1)]
    all_to_all x1 -> x0, starting transfers between devices: 5.23 us -> none  [local(): lax.all_to_all(results, ('sp', 'tp'), split_axis=0, concat_axis=0, tiled=...]
    dot_general x0 -> x1, matrix products: none -> 4.24 us  [local(): both_out = jnp.dot(both, flat_back, preferred_element_type=jnp.float32)]
  transfers between devices with their start and end apart: 3 -> 2, of which waited for: 2 -> 1; matrix products, arithmetic and copies ran while one was open for 9% -> 9% of each run, Pallas kernels for 0% -> 0%
where the time goes in v2:
time: 273 us
  Pallas kernels  168 us (62%)
  matrix products  37.8 us (14%)
  blocking collectives  27 us (10%)
  between operations  13.6 us (5%)
  local copies, waits for them, and re-layouts  12.8 us (5%)
  starting transfers between devices  8.72 us (3%)
  other arithmetic  3.12 us (1%)
    pallas_call x2, Pallas kernels, exchange(): pl.pallas_call(functools.partial(exchange_kernel, n_sp, n_tp), out_shape=...  168 us
    all_gather x1, blocking collectives, local(): lax.all_gather(key_rows, 'sp', axis=0, tiled=True)  13.9 us
    all_gather x1, blocking collectives, local(): lax.all_gather(value_rows, 'sp', axis=0, tiled=True)  13.1 us
    all_to_all x1, starting transfers between devices, local(): lax.all_to_all(attended, 'tp', split_axis=0, concat_axis=1, tiled=True)  8.72 us
    dot_general x1, matrix products, local(): jnp.dot(hidden, down_weight[0], preferred_element_type=jnp.float32)  7.75 us
    reshape x2, local copies, waits for them, and re-layouts, visit(): score = score.reshape(shard_len, heads_here, blocks_per, KBLK)  5.64 us
  transfers between devices with their start and end apart: 2, of which 1 were waited for; matrix products, arithmetic and copies ran while one was open for 9% of the time, Pallas kernels for 0%

profile of v2, /device:TPU:11, one launch (start us, length us, event | category | flops | bytes accessed | tf_op | source)
XLA Modules:
  0.0 272.7 jit_solution(9450224639837039384)
XLA Ops:
  6.5 0.7 all-gather.2.cloned.1.call-update
  7.3 13.9 %all_gather.10 = bf16[2048,128]{1,0:T(8,128)(2,1)} all-gather(bf16[512,128]{1,0:T(8,128)(2,1)} %param.20), channel_id=1, replica_groups=mesh['grp'=2,'sp'=4,'tp'=4] {'sp'}, dimensions={0}, use_global_device_ids=true | all-gather | bytes 655360 | tf_op jit(solution)/shard_map/all_gather | solution.py:156
  21.2 13.1 %all_gather.9 = bf16[2048,128]{1,0:T(8,128)(2,1)S(1)} all-gather(bf16[512,128]{1,0:T(8,128)(2,1)} %param.21), channel_id=1, replica_groups=mesh['grp'=2,'sp'=4,'tp'=4] {'sp'}, dimensions={0}, use_global_device_ids=true | all-gather | bytes 655360 | tf_op jit(solution)/shard_map/all_gather | solution.py:157
  34.4 22.5 %while.15 = (s32[]{:T(128)}, f32[512,1,128]{0,2,1:T(8,128)S(1)}, f32[512,1]{0,1:T(1,128)S(1)}, s32[]{:T(128)}, s32[]{:T(128)}, /*index=5*/bf16[2048,128]{1,0:T(8...) while((s32[]{:T(128)}, f32[512,1,128]{0,2,1:T(8,128)S(1)}, ...), condition=%wide.region_3.4_spmd.clone, body=%wide.region_0.3_spmd.clone.sunk | while | flops 1081683968 | bytes 25510100 | solution.py:72
  34.4 2.7 convolution_multiply_fusion.5
  37.1 2.9 %copy.83 = f32[512,1,1024]{2,0,1:T(8,128)} copy(f32[512,1,1024]{0,2,1:T(8,128)} %bitcast.105) | data formatting | bytes 4194304 | tf_op jit(solution)/shard_map/while/body/mul | solution.py:47
  40.0 2.7 %reshape.239 = f32[4096,128]{1,0:T(8,128)} reshape(f32[512,1,1024]{2,0,1:T(8,128)} %copy.83) | data formatting | bytes 4194304 | tf_op jit(solution)/shard_map/while/body/reshape | solution.py:50
  42.9 0.2 lt.96
  43.0 5.3 %fusion.96 = f32[4096,128]{1,0:T(8,128)} fusion(f32[4096,128]{1,0:T(8,128)} %reshape.239, s32[4096]{0:T(1024)S(1)} %lt.96, s32[8,128]{1,0:T(8,128)S(1)} %add_add_fusion.2), kind=kOutput, calls=%fused_computation.4.clone.1 | convolution fusion | flops 809533440 | bytes 4214784 | tf_op jit(solution)/shard_map/while/body/dot_general | solution.py:53
  48.3 2.2 copy.84
  50.6 2.9 %copy.82 = f32[512,8,128]{2,0,1:T(8,128)} copy(f32[512,8,128]{0,2,1:T(8,128)} %bitcast.106) | data formatting | bytes 4194304 | tf_op jit(solution)/shard_map/while/body/reshape | solution.py:50
  53.5 3.2 %fusion.98 = f32[512,128]{0,1:T(8,128)S(1)} fusion(bf16[8,128,128]{2,1,0:T(8,128)(2,1)S(1)} %bitcast.109, f32[512,8,128]{2,0,1:T(8,128)} %copy.82, f32[512,8,128]{2,1,0:T(8,128)} %bitcast.108, f32[512,8]{0,1:T(8,128)S(1)} %fusion.97, s32[8,128]{1,0:T(8,128)S(1)} %add_add_fusion.2, s32[512]{0:T(512)S(1)} %iota_add_fusion.2), kind=kOutput, calls=%fused_computation.6.clone.1 | convolution fusion | flops 137297920 | bytes 4741120 | tf_op jit(solution)/shard_map/while/body/qhbk,bkhd->qhbd/dot_general | solution.py:58
  56.9 0.8 copy.63
  57.6 8.7 %all-to-all-start = ((bf16[4,128,128]{2,1,0:T(8,128)(2,1)}), bf16[4,128,128]{2,1,0:T(8,128)(2,1)S(1)}, u32[]{:S(2)}, u32[]{:S(2)}) async-start(bf16[4,128,128]{2,1,0:T(8,128)(2,1)} %bitcast.1), calls=%async_computation | async-start | bytes 262144 | tf_op jit(solution)/shard_map/all_to_all | solution.py:162
  66.6 0.3 fusion.36
  67.0 0.2 select_reduce_fusion
  67.3 0.8 fusion.33
  68.2 0.5 all-to-all-done
  68.9 2.1 fusion.65
  71.0 0.3 multiply_reduce_fusion.1
  71.3 0.2 add_convert_fusion.1
  71.6 0.4 copy-done.4
  71.9 2.7 convolution_convert_fusion.1
  74.6 96.1 %shard_map.163 = bf16[16,48,2048]{2,1,0:T(8,128)(2,1)} custom-call(bf16[16,48,2048]{2,1,0:T(8,128)(2,1)} %bitcast.110), custom_call_target="tpu_custom_call" | custom-call | tf_op jit(solution)/shard_map/pallas_call | solution.py:119
  170.7 4.0 %fusion.41 = f32[768,256]{1,0:T(8,128)} fusion(bf16[768,2048]{1,0:T(8,128)(2,1)} %bitcast.113, bf16[1,2048,256]{2,1,0:T(8,128)(2,1)} %param.28), kind=kOutput, calls=%fused_computation.59 | convolution fusion | flops 805306368 | bytes 4980736 | tf_op jit(solution)/shard_map/dot_general | solution.py:194
  174.7 7.8 %convolution_convert_fusion = bf16[768,2048]{1,0:T(8,128)(2,1)} fusion(bf16[768,2048]{1,0:T(8,128)(2,1)} %bitcast.114, bf16[1,256,2048]{2,1,0:T(8,128)(2,1)} %param.30, bf16[1,2048,256]{2,1,0:T(8,128)(2,1)} %param.29, f32[768,256]{1,0:T(8,128)} %fusion.41), kind=kOutput, calls=%fused_computation.41 | convolution fusion | flops 1613365248 | bytes 9175040 | tf_op jit(solution)/shard_map/dot_general | solution.py:197
  182.5 72.3 %shard_map.164 = bf16[16,48,2048]{2,1,0:T(8,128)(2,1)} custom-call(bf16[16,48,2048]{2,1,0:T(8,128)(2,1)} %bitcast.115), custom_call_target="tpu_custom_call" | custom-call | tf_op jit(solution)/shard_map/pallas_call | solution.py:119
  254.7 2.0 fusion.67
  256.8 4.2 %fusion.49 = f32[256,2048]{1,0:T(8,128)} fusion(bf16[768,2048]{1,0:T(8,128)(2,1)} %bitcast.111, bf16[128,768]{1,0:T(8,128)(2,1)S(1)} %get-tuple-element.161, bf16[128,768]{1,0:T(8,128)(2,1)S(1)} %get-tuple-element.160), kind=kOutput, calls=%fused_computation.74 | convolution fusion | flops 806092800 | bytes 5636096 | tf_op jit(solution)/shard_map/dot_general | solution.py:209
  261.0 3.5 %fusion.66 = (f32[128]{0:T(128)S(1)}, f32[128,2048]{1,0:T(8,128)S(1)}) fusion(bf16[512,2048]{1,0:T(8,128)(2,1)S(1)} %copy-done, bf16[128,2048]{1,0:T(8,128)(2,1)} %copy-done.1, bf16[2048,512]{1,0:T(8,128)(2,1)} %param.32, f32[128,512]{1,0:T(8,128)S(1)} %fusion.67, f32[256,2048]{1,0:T(8,128)} %fusion.49), kind=kOutput, calls=%fused_computation.97 | convolution fusion | flops 538574720 | bytes 8651264 | tf_op jit(solution)/shard_map/dot_general | solution.py:214
  264.6 0.3 multiply_reduce_fusion
  264.8 1.0 add_convert_fusion
  (46 shorter events, 1.0 us)
Async XLA Ops:
  6.5 254.5 %copy-start = (bf16[512,2048]{1,0:T(8,128)(2,1)S(1)}, bf16[512,2048]{1,0:T(8,128)(2,1)}, u32[]{:S(2)}) copy-start(bf16[512,2048]{1,0:T(8,128)(2,1)} %param.33) | copy-start | bytes 6291460
  6.5 27.8 %copy-start.2 = (bf16[512,128]{1,0:T(8,128)(2,1)S(1)}, bf16[512,128]{1,0:T(8,128)(2,1)}, u32[]{:S(2)}) copy-start(bf16[512,128]{1,0:T(8,128)(2,1)} %param.19) | copy-start | bytes 393220
  6.5 62.3 %all-gather.2.cloned.1.call-start = ((), (), s32[]{:S(2)}) async-start(), calls=%async_computation.1 | async-start | bytes 2621440 | tf_op jit(solution)/shard_map/all_gather | solution.py:165
  34.3 32.0 %copy-start.9 = (s32[128,4]{0,1:T(4,128)S(1)}, s32[128,4]{0,1:T(4,128)}, u32[]{:S(2)}) copy-start(s32[128,4]{0,1:T(4,128)} %param.26) | copy-start | bytes 6148
  34.3 32.7 %copy-start.10 = (f32[128,4]{0,1:T(4,128)S(1)}, f32[128,4]{0,1:T(4,128)}, u32[]{:S(2)}) copy-start(f32[128,4]{0,1:T(4,128)} %param.27) | copy-start | bytes 6148
  56.8 12.0 %copy-start.3 = (bf16[128,2048]{1,0:T(8,128)(2,1)S(1)}, bf16[128,2048]{1,0:T(8,128)(2,1)}, u32[]{:S(2)}) copy-start(bf16[128,2048]{1,0:T(8,128)(2,1)} %param.22) | copy-start | bytes 1572868
  57.6 11.0 %all-to-all-start = ((bf16[4,128,128]{2,1,0:T(8,128)(2,1)}), bf16[4,128,128]{2,1,0:T(8,128)(2,1)S(1)}, u32[]{:S(2)}, u32[]{:S(2)}) async-start(bf16[4,128,128]{2,1,0:T(8,128)(2,1)} %bitcast.1), calls=%async_computation | async-start | bytes 262144 | tf_op jit(solution)/shard_map/all_to_all | solution.py:162
  68.8 2.5 copy-start.5
  68.8 2.5 copy-start.6
  71.0 0.9 copy-start.4
  71.9 182.8 %copy-start.1 = (bf16[128,2048]{1,0:T(8,128)(2,1)}, bf16[128,2048]{1,0:T(8,128)(2,1)S(1)}, u32[]{:S(2)}) copy-start(bf16[128,2048]{1,0:T(8,128)(2,1)S(1)} %add_convert_fusion.1) | copy-start | bytes 1572868
  261.0 3.8 %copy-start.7 = (f32[2048]{0:T(1024)S(1)}, f32[2048]{0:T(1024)}, u32[]{:S(2)}) copy-start(f32[2048]{0:T(1024)} %param.35) | copy-start | bytes 24580
  261.0 3.8 %copy-start.8 = (f32[2048]{0:T(1024)S(1)}, f32[2048]{0:T(1024)}, u32[]{:S(2)}) copy-start(f32[2048]{0:T(1024)} %param.34) | copy-start | bytes 24580
Sparse Core Ops, SparseCore 0:
  8.9 23.1 all-gather.1

commit v3 on v2

--- a/solution.py
+++ b/solution.py
@@ -21,56 +21,226 @@
     return centred * lax.rsqrt(spread + NORM_EPS) * gains + offset
 
 
-def stick_local(query_rows, key_all, value_all, seq_index):
-    shard_len = query_rows.shape[0]
-    heads_here = query_rows.shape[1] // HEAD_DIM
-    step_len = 2 * shard_len
-    blocks_per = step_len // KBLK
+def three_parts(exact):
+    high = exact.astype(jnp.bfloat16)
+    rest = exact - high.astype(jnp.float32)
+    middle = rest.astype(jnp.bfloat16)
+    low = (rest - middle.astype(jnp.float32)).astype(jnp.bfloat16)
+    return jnp.concatenate([high, middle, low], axis=1)
+
+
+def mixer_kernel(
+    n_sp,
+    n_tp,
+    query_ref,
+    key_ref,
+    value_ref,
+    weight_ref,
+    parts_ref,
+    weights_ref,
+    held,
+    summed,
+    behind,
+    ready,
+    held_send,
+    held_recv,
+    weight_send,
+    weight_recv,
+    part_send,
+    part_recv,
+    own_sem,
+):
+    mesh_ids = pl.DeviceIdType.MESH
+    seq_index, tp_index = lax.axis_index("sp"), lax.axis_index("tp")
+    shard_len, features = query_ref.shape
+    tokens = shard_len // n_tp
+    heads = features // HEAD_DIM
+    tile = min(shard_len, 256)
     scale = HEAD_DIM ** (-0.5)
-    queries = query_rows.reshape(shard_len, heads_here, HEAD_DIM)
-    query_pos = seq_index * shard_len + jnp.arange(shard_len, dtype=jnp.int32)
-    visits = seq_index // 2 + 1
-    upper = (jnp.arange(KBLK)[:, None] >= jnp.arange(KBLK)[None, :]).astype(jnp.float32)
-
-    def visit(visit_no, carry):
-        summed, behind = carry
-        chosen = visits - 1 - visit_no
-        first_key = chosen * step_len
-        key_block = lax.dynamic_slice_in_dim(key_all, first_key, step_len, 0).reshape(
-            step_len, heads_here, HEAD_DIM
-        )
-        value_block = lax.dynamic_slice_in_dim(value_all, first_key, step_len, 0).reshape(
-            blocks_per, KBLK, heads_here, HEAD_DIM
-        )
-        key_pos = (first_key + jnp.arange(step_len, dtype=jnp.int32)).reshape(blocks_per, KBLK)
-        score = (
-            jnp.einsum("qhd,khd->qhk", queries, key_block, preferred_element_type=jnp.float32)
-            * scale
-        )
-        score = score.reshape(shard_len, heads_here, blocks_per, KBLK)
-        usable = key_pos[None, None, :, :] < query_pos[:, None, None, None]
-        spent = jnp.where(usable, jax.nn.softplus(score), 0.0)
-        inside = jnp.dot(spent.reshape(-1, KBLK), upper, precision=lax.Precision.HIGHEST).reshape(
-            spent.shape
-        )
-        totals = inside[..., 0]
-        weight = jnp.where(usable, jnp.exp(score - inside), 0.0).astype(jnp.bfloat16)
-        pieces = jnp.einsum(
-            "qhbk,bkhd->qhbd", weight, value_block, preferred_element_type=jnp.float32
-        )
-        block_running = jnp.cumsum(totals, axis=-1)
-        step_total = block_running[..., -1]
-        beyond = step_total[..., None] - block_running
-        factor = jnp.exp(-(behind[..., None] + beyond))
-        summed = summed + jnp.sum(pieces * factor[..., None], axis=2)
-        return (summed, behind + step_total)
-
-    initial = (
-        jnp.zeros((shard_len, heads_here, HEAD_DIM), jnp.float32),
-        jnp.zeros((shard_len, heads_here), jnp.float32),
-    )
-    summed, _ = lax.fori_loop(0, visits, visit, initial)
-    return summed.reshape(shard_len, heads_here * HEAD_DIM).astype(jnp.bfloat16)
+    has_next, has_last = seq_index < n_sp - 1, seq_index > 0
+    after, ahead = lax.rem(seq_index + 1, n_sp), lax.rem(seq_index + n_sp - 1, n_sp)
+
+    barrier = pltpu.get_barrier_semaphore()
+
+    @pl.when(has_next)
+    def _():
+        pl.semaphore_signal(barrier, inc=1, device_id={"sp": after}, device_id_type=mesh_ids)
+
+    @pl.when(has_last)
+    def _():
+        pl.semaphore_signal(barrier, inc=1, device_id={"sp": ahead}, device_id_type=mesh_ids)
+
+    for step in range(1, n_tp):
+        peer = lax.rem(tp_index + step, n_tp)
+        pl.semaphore_signal(barrier, inc=1, device_id={"tp": peer}, device_id_type=mesh_ids)
+
+    own_copies = [
+        pltpu.make_async_copy(key_ref, held.at[seq_index, 0], own_sem.at[0]),
+        pltpu.make_async_copy(value_ref, held.at[seq_index, 1], own_sem.at[1]),
+        pltpu.make_async_copy(weight_ref, weights_ref.at[tp_index], own_sem.at[2]),
+    ]
+    for copy in own_copies:
+        copy.start()
+    summed[...] = jnp.zeros_like(summed)
+    behind[...] = jnp.zeros_like(behind)
+    pl.semaphore_wait(
+        barrier, n_tp - 1 + has_next.astype(jnp.int32) + has_last.astype(jnp.int32)
+    )
+
+    def held_copy(step, which):
+        block = lax.rem(seq_index - step + n_sp, n_sp)
+        return pltpu.make_async_remote_copy(
+            src_ref=held.at[block, which],
+            dst_ref=held.at[block, which],
+            send_sem=held_send.at[step, which],
+            recv_sem=held_recv.at[step, which],
+            device_id={"sp": after},
+            device_id_type=mesh_ids,
+        )
+
+    def arrived(step, which):
+        block = lax.rem(seq_index - step + n_sp, n_sp)
+        return pltpu.make_async_remote_copy(
+            src_ref=held.at[block, which],
+            dst_ref=held.at[block, which],
+            send_sem=held_send.at[step - 1, which],
+            recv_sem=held_recv.at[step - 1, which],
+            device_id={"sp": after},
+            device_id_type=mesh_ids,
+        )
+
+    def weight_copy(step, landing):
+        return pltpu.make_async_remote_copy(
+            src_ref=weight_ref,
+            dst_ref=weights_ref.at[landing],
+            send_sem=weight_send.at[step],
+            recv_sem=weight_recv.at[step],
+            device_id={"tp": lax.rem(tp_index + step, n_tp)},
+            device_id_type=mesh_ids,
+        )
+
+    def part_copy(step, landing):
+        peer = lax.rem(tp_index + step, n_tp)
+        return pltpu.make_async_remote_copy(
+            src_ref=ready.at[peer],
+            dst_ref=parts_ref.at[landing],
+            send_sem=part_send.at[step],
+            recv_sem=part_recv.at[step],
+            device_id={"tp": peer},
+            device_id_type=mesh_ids,
+        )
+
+    for copy in own_copies:
+        copy.wait()
+
+    @pl.when(has_next)
+    def _():
+        for which in range(2):
+            held_copy(0, which).start()
+
+    for step in range(1, n_tp):
+        weight_copy(step, tp_index).start()
+
+    key_lane = lax.broadcasted_iota(jnp.int32, (tile, KBLK), 1)
+    query_row = lax.broadcasted_iota(jnp.int32, (tile, KBLK), 0)
+    from_row = lax.broadcasted_iota(jnp.int32, (KBLK, 2 * KBLK), 0)
+    to_lane = lax.broadcasted_iota(jnp.int32, (KBLK, 2 * KBLK), 1)
+    reach = ((from_row >= to_lane) | (to_lane >= KBLK)).astype(jnp.float32).astype(jnp.bfloat16)
+    reach = jnp.concatenate([reach, reach, reach], axis=0)
+
+    @pl.loop(0, seq_index + 1)
+    def _(step):
+        @pl.when(step > 0)
+        def _():
+            for which in range(2):
+                arrived(step, which).wait_recv()
+
+            @pl.when(has_next)
+            def _():
+                for which in range(2):
+                    held_copy(step, which).start()
+
+        block = seq_index - step
+        for head in range(heads):
+            lanes = slice(head * HEAD_DIM, (head + 1) * HEAD_DIM)
+            for first_key in reversed(range(0, shard_len, KBLK)):
+                key_block = held[block, 0, first_key : first_key + KBLK, lanes]
+                value_block = held[block, 1, first_key : first_key + KBLK, lanes]
+                for first_query in range(0, shard_len, tile):
+                    rows = slice(first_query, first_query + tile)
+                    score = scale * lax.dot_general(
+                        query_ref[rows, lanes],
+                        key_block,
+                        (((1,), (1,)), ((), ())),
+                        preferred_element_type=jnp.float32,
+                    )
+                    usable = (key_lane + first_key) < (
+                        query_row + (first_query + step * shard_len)
+                    )
+                    grown = jnp.maximum(score, 0.0) + jnp.log(1.0 + jnp.exp(-jnp.abs(score)))
+                    spent = jnp.where(usable, grown, 0.0)
+                    sums = jnp.dot(three_parts(spent), reach, preferred_element_type=jnp.float32)
+                    share = jnp.where(usable, jnp.exp(score - sums[:, :KBLK]), 0.0)
+                    piece = jnp.dot(
+                        share.astype(jnp.bfloat16),
+                        value_block,
+                        preferred_element_type=jnp.float32,
+                    )
+                    before = behind[head, rows, :]
+                    summed[rows, lanes] += piece * jnp.exp(-before)
+                    behind[head, rows, :] = before + sums[:, KBLK:]
+
+    for peer in range(n_tp):
+        ready[peer] = summed[peer * tokens : (peer + 1) * tokens, :].astype(jnp.bfloat16)
+    for step in range(1, n_tp):
+        part_copy(step, tp_index).start()
+    parts_ref[tp_index] = ready[tp_index]
+
+    @pl.when(has_next)
+    def _():
+        @pl.loop(0, seq_index + 1)
+        def _(step):
+            for which in range(2):
+                held_copy(step, which).wait_send()
+
+    for step in range(1, n_tp):
+        source = lax.rem(tp_index + n_tp - step, n_tp)
+        weight_copy(step, source).wait()
+        part_copy(step, source).wait()
+
+
+def mixer(query_rows, key_rows, value_rows, output_weight):
+    n_sp, n_tp = lax.axis_size("sp"), lax.axis_size("tp")
+    shard_len, features = query_rows.shape
+    tokens = shard_len // n_tp
+    heads = features // HEAD_DIM
+    in_vmem = pl.BlockSpec(memory_space=pltpu.VMEM)
+    dma = pltpu.SemaphoreType.DMA
+    parts, weights = pl.pallas_call(
+        functools.partial(mixer_kernel, n_sp, n_tp),
+        out_shape=(
+            jax.ShapeDtypeStruct((n_tp, tokens, features), jnp.bfloat16),
+            jax.ShapeDtypeStruct((n_tp,) + output_weight.shape, output_weight.dtype),
+        ),
+        in_specs=[in_vmem] * 4,
+        out_specs=(in_vmem, in_vmem),
+        scratch_shapes=[
+            pltpu.VMEM((n_sp, 2, shard_len, features), jnp.bfloat16),
+            pltpu.VMEM((shard_len, features), jnp.float32),
+            pltpu.VMEM((heads, shard_len, KBLK), jnp.float32),
+            pltpu.VMEM((n_tp, tokens, features), jnp.bfloat16),
+            dma((n_sp, 2)),
+            dma((n_sp, 2)),
+            dma((n_tp,)),
+            dma((n_tp,)),
+            dma((n_tp,)),
+            dma((n_tp,)),
+            dma((3,)),
+        ],
+        compiler_params=pltpu.CompilerParams(collective_id=3, has_side_effects=True),
+    )(query_rows, key_rows, value_rows, output_weight)
+    by_token = jnp.concatenate([parts[index] for index in range(n_tp)], axis=1)
+    return by_token, weights.reshape(-1, output_weight.shape[1])
 
 
 def exchange_kernel(n_sp, n_tp, src, dst, send_sem, recv_sem, own_sem):
@@ -151,20 +321,10 @@
     second_gain,
     second_bias,
 ):
-    seq_index = lax.axis_index("sp")
-    key_all, value_all = (
-        lax.all_gather(key_rows, "sp", axis=0, tiled=True),
-        lax.all_gather(value_rows, "sp", axis=0, tiled=True),
-    )
-    attended = stick_local(query_rows, key_all, value_all, seq_index)
+    by_token, weights = mixer(query_rows, key_rows, value_rows, output_weight)
     tokens_here = residual.shape[0]
     width = residual.shape[1]
-    by_token = lax.all_to_all(attended, "tp", split_axis=0, concat_axis=1, tiled=True)
-    mixed = jnp.dot(
-        by_token,
-        lax.all_gather(output_weight, "tp", axis=0, tiled=True),
-        preferred_element_type=jnp.float32,
-    )
+    mixed = jnp.dot(by_token, weights, preferred_element_type=jnp.float32)
     normed = layer_norm(residual.astype(jnp.float32) + mixed, first_gain, first_bias).astype(
         jnp.bfloat16
     )
@@ -198,7 +358,7 @@
         jnp.bfloat16
     )
     results = produced.reshape(slot_rows.shape)
-    returned = exchange(results, 2)
+    returned = lax.all_to_all(results, ("sp", "tp"), split_axis=0, concat_axis=0, tiled=True)
     flat_back = returned.reshape(experts * capacity, width)
     placed = slot_ids.reshape(tokens_here, top_count)[:, :, None] == jnp.arange(
         experts * capacity, dtype=jnp.int32

time: 273 us -> 208 us (0.76)
  waiting for transfers between devices: 1.21 us -> 67.7 us
  Pallas kernels: 168 us -> 103 us
  blocking collectives: 27 us -> 0 us
  between operations: 13.6 us -> 0.19 us
  matrix products: 37.8 us -> 26.5 us
  local copies, waits for them, and re-layouts: 12.8 us -> 2.03 us
  starting transfers between devices: 8.72 us -> 5.83 us
    pallas_call x2 -> x1, Pallas kernels: 168 us -> 72.9 us  [exchange(): pl.pallas_call(functools.partial(exchange_kernel, n_sp, n_tp), out_shape=...]
    all_to_all x1, waiting for transfers between devices: 0.47 us -> 67.7 us  [local(): lax.all_to_all(results, ('sp', 'tp'), split_axis=0, concat_axis=0, tiled=...]
    pallas_call x0 -> x1, Pallas kernels: none -> 30 us  [mixer(): pl.pallas_call(functools.partial(mixer_kernel, n_sp, n_tp), out_shape=(ja...]
    all_gather x2 -> x0, blocking collectives: 27 us -> none  [the longest x1 13.9 us: local(): lax.all_gather(key_rows, 'sp', axis=0, tiled=True)]
    dot_general x4 -> x1, matrix products: 13.3 us -> 2.21 us  [local(): mixed = jnp.dot(by_token, weights, preferred_element_type=jnp.float32)]
    reshape x2 -> x0, local copies, waits for them, and re-layouts: 5.64 us -> none  [visit(): score = score.reshape(shard_len, heads_here, blocks_per, KBLK)]
    while x2 -> x0, local copies, waits for them, and re-layouts: 2.96 us -> none
    mul x1 -> x0, local copies, waits for them, and re-layouts: 2.93 us -> none  [visit(): jnp.einsum('qhd,khd->qhk', queries, key_block, preferred_element_type=jnp...]
  transfers between devices with their start and end apart: 2 -> 1, of which waited for: 1 -> 1; matrix products, arithmetic and copies ran while one was open for 9% -> 1% of each run, Pallas kernels for 0% -> 0%
where the time goes in v3:
time: 208 us; the launch traced here: 207 us
  Pallas kernels  103 us (50%)
  waiting for transfers between devices  67.7 us (33%)
  matrix products  26.5 us (13%)
  starting transfers between devices  5.83 us (3%)
  other arithmetic  2.34 us (1%)
    pallas_call x1, Pallas kernels, exchange(): pl.pallas_call(functools.partial(exchange_kernel, n_sp, n_tp), out_shape=...  72.9 us
    all_to_all x1, waiting for transfers between devices, local(): lax.all_to_all(results, ('sp', 'tp'), split_axis=0, concat_axis=0, tiled=...  67.7 us
    pallas_call x1, Pallas kernels, mixer(): pl.pallas_call(functools.partial(mixer_kernel, n_sp, n_tp), out_shape=(ja...  30 us
    dot_general x1, matrix products, local(): jnp.dot(hidden, down_weight[0], preferred_element_type=jnp.float32)  7.75 us
    all_to_all x1, starting transfers between devices, local(): lax.all_to_all(results, ('sp', 'tp'), split_axis=0, concat_axis=0, tiled=...  5.83 us
    dot_general x1, matrix products, local(): both_out = jnp.dot(both, flat_back, preferred_element_type=jnp.float32)  4.24 us
  transfers between devices with their start and end apart: 1, of which 1 were waited for; matrix products, arithmetic and copies ran while one was open for 1% of the time, Pallas kernels for 0%

profile of v3, /device:TPU:11, one launch (start us, length us, event | category | flops | bytes accessed | tf_op | source)
XLA Modules:
  0.0 207.3 jit_solution(18129269936877675497)
XLA Ops:
  0.0 0.0 copy-start
  0.0 30.0 %shard_map.163 = (bf16[4,128,128]{2,1,0:T(8,128)(2,1)}, bf16[4,128,2048]{2,1,0:T(8,128)(2,1)}) custom-call(bf16[512,128]{1,0:T(8,128)(2,1)} %query_ref.1, bf16[512,128]{1,0:T(8,128)(2,1)} %key_ref.1, bf16[512,128]{1,0:T(8,128)(2,1)} %value_ref.1, bf16[128,2048]{1,0:T(8,128)(2,1)} %weight_ref.1), custom_call_target="tpu_custom_call" | custom-call | tf_op jit(solution)/shard_map/pallas_call | solution.py:219
  30.0 0.8 slice_bitcast_fusion.3
  30.8 0.0 copy-start.7
  30.8 0.0 copy-start.3
  30.8 0.0 copy-start.4
  30.8 2.2 %fusion.40 = (f32[128]{0:T(128)S(1)}, f32[128,2048]{1,0:T(8,128)S(1)}) fusion(bf16[512,2048]{1,0:T(8,128)(2,1)} %bitcast.38, bf16[128,128]{1,0:T(8,128)(2,1)S(1)} %get-tuple-element.12, bf16[128,128]{1,0:T(8,128)(2,1)S(1)} %get-tuple-element.13, bf16[128,128]{1,0:T(8,128)(2,1)S(1)} %get-tuple-element.14, bf16[128,128]{1,0:T(8,128)(2,1)S(1)} %get-tuple-element.11, ...), kind=kOutput, calls=%fused_computation.67 | convolution fusion | flops 269746048 | bytes 3801600 | tf_op jit(solution)/shard_map/dot_general | solution.py:327
  33.1 0.3 multiply_reduce_fusion.1
  33.3 0.0 copy-done.7
  33.3 0.1 copy.30
  33.4 0.1 eq.20
  33.6 0.3 fusion.3
  33.8 0.1 convert_element_type.49
  34.0 0.1 copy.31
  34.0 0.2 fusion
  34.3 0.0 copy-done.3
  34.3 0.2 add_convert_fusion.1
  34.5 0.0 copy-start.1
  34.5 0.8 copy-done.1
  35.3 2.7 %convolution_convert_fusion.1 = bf16[768,2048]{1,0:T(8,128)(2,1)} fusion(pred[768,128]{1,0:T(8,128)(4,1)S(1)} %fusion, bf16[128,2048]{1,0:T(8,128)(2,1)S(1)} %add_convert_fusion.1), kind=kOutput, calls=%fused_computation.1 | convolution fusion | flops 404226048 | bytes 3768320 | tf_op jit(solution)/shard_map/dot_general | solution.py:350
  38.0 72.9 %shard_map.164 = bf16[16,48,2048]{2,1,0:T(8,128)(2,1)} custom-call(bf16[16,48,2048]{2,1,0:T(8,128)(2,1)} %bitcast.34), custom_call_target="tpu_custom_call" | custom-call | tf_op jit(solution)/shard_map/pallas_call | solution.py:289
  110.9 3.8 %fusion.8 = f32[768,256]{1,0:T(8,128)} fusion(bf16[768,2048]{1,0:T(8,128)(2,1)} %bitcast.36, bf16[1,2048,256]{2,1,0:T(8,128)(2,1)S(1)} %copy-done.9), kind=kOutput, calls=%fused_computation.18 | convolution fusion | flops 805306368 | bytes 4980736 | tf_op jit(solution)/shard_map/dot_general | solution.py:354
  114.7 7.8 %convolution_convert_fusion = bf16[768,2048]{1,0:T(8,128)(2,1)} fusion(bf16[768,2048]{1,0:T(8,128)(2,1)} %bitcast.37, bf16[1,256,2048]{2,1,0:T(8,128)(2,1)} %param.28, bf16[1,2048,256]{2,1,0:T(8,128)(2,1)} %param.27, f32[768,256]{1,0:T(8,128)} %fusion.8), kind=kOutput, calls=%fused_computation | convolution fusion | flops 1613365248 | bytes 9175040 | tf_op jit(solution)/shard_map/dot_general | solution.py:357
  122.4 5.8 %all-to-all-start = ((bf16[16,48,2048]{2,1,0:T(8,128)(2,1)}), bf16[16,48,2048]{2,1,0:T(8,128)(2,1)}, u32[]{:S(2)}, u32[]{:S(2)}) async-start(bf16[16,48,2048]{2,1,0:T(8,128)(2,1)} %bitcast.35), calls=%async_computation | async-start | bytes 6291456 | tf_op jit(solution)/shard_map/all_to_all | solution.py:361
  128.3 0.2 select_reduce_fusion
  128.5 2.0 fusion.42
  130.6 67.7 %all-to-all-done = bf16[16,48,2048]{2,1,0:T(8,128)(2,1)} async-done(((bf16[16,48,2048]{2,1,0:T(8,128)(2,1)}), bf16[16,48,2048]{2,1,0:T(8,128)(2,1)}, u32[]{:S(2)}, u32[]{:S(2)}) %all-to-all-start) | async-done | bytes 3145760 | tf_op jit(solution)/shard_map/all_to_all | solution.py:361
  198.2 4.2 %fusion.16 = f32[256,2048]{1,0:T(8,128)} fusion(bf16[768,2048]{1,0:T(8,128)(2,1)} %bitcast.11, bf16[128,768]{1,0:T(8,128)(2,1)S(1)} %get-tuple-element.10, bf16[128,768]{1,0:T(8,128)(2,1)S(1)} %get-tuple-element.9), kind=kOutput, calls=%fused_computation.33 | convolution fusion | flops 806092800 | bytes 5636096 | tf_op jit(solution)/shard_map/dot_general | solution.py:369
  202.5 0.0 copy-done
  202.5 3.5 %fusion.41 = (f32[128]{0:T(128)S(1)}, f32[128,2048]{1,0:T(8,128)S(1)}) fusion(bf16[512,2048]{1,0:T(8,128)(2,1)S(1)} %copy-done, bf16[128,2048]{1,0:T(8,128)(2,1)} %copy-done.1, bf16[2048,512]{1,0:T(8,128)(2,1)} %param.30, f32[128,512]{1,0:T(8,128)S(1)} %fusion.42, f32[256,2048]{1,0:T(8,128)} %fusion.16), kind=kOutput, calls=%fused_computation.68 | convolution fusion | flops 538574720 | bytes 8651264 | tf_op jit(solution)/shard_map/dot_general | solution.py:374
  206.0 0.3 multiply_reduce_fusion
  206.3 1.0 add_convert_fusion
  (18 shorter events, 0.1 us)
Async XLA Ops:
  0.0 202.5 %copy-start = (bf16[512,2048]{1,0:T(8,128)(2,1)S(1)}, bf16[512,2048]{1,0:T(8,128)(2,1)}, u32[]{:S(2)}) copy-start(bf16[512,2048]{1,0:T(8,128)(2,1)} %param.31) | copy-start | bytes 6291460
  30.8 2.5 %copy-start.7 = (s32[128,4]{0,1:T(4,128)S(1)}, s32[128,4]{0,1:T(4,128)}, u32[]{:S(2)}) copy-start(s32[128,4]{0,1:T(4,128)} %param.24) | copy-start | bytes 6148
  30.8 3.5 %copy-start.3 = (f32[2048]{0:T(1024)S(1)}, f32[2048]{0:T(1024)}, u32[]{:S(2)}) copy-start(f32[2048]{0:T(1024)} %param.23) | copy-start | bytes 24580
  30.8 3.5 %copy-start.4 = (f32[2048]{0:T(1024)S(1)}, f32[2048]{0:T(1024)}, u32[]{:S(2)}) copy-start(f32[2048]{0:T(1024)} %param.22) | copy-start | bytes 24580
  34.5 0.8 copy-start.1
  38.0 72.9 %copy-start.9 = (bf16[1,2048,256]{2,1,0:T(8,128)(2,1)S(1)}, bf16[1,2048,256]{2,1,0:T(8,128)(2,1)}, u32[]{:S(2)}) copy-start(bf16[1,2048,256]{2,1,0:T(8,128)(2,1)} %param.26) | copy-start | bytes 3145732
  122.4 5.8 %copy-start.8 = (f32[128,4]{0,1:T(4,128)S(1)}, f32[128,4]{0,1:T(4,128)}, u32[]{:S(2)}) copy-start(f32[128,4]{0,1:T(4,128)} %param.25) | copy-start | bytes 6148
  122.4 6.1 %copy-start.2 = (bf16[128,2048]{1,0:T(8,128)(2,1)S(1)}, bf16[128,2048]{1,0:T(8,128)(2,1)}, u32[]{:S(2)}) copy-start(bf16[128,2048]{1,0:T(8,128)(2,1)} %copy-done.1) | copy-start | bytes 1572868
  122.4 75.8 %all-to-all-start = ((bf16[16,48,2048]{2,1,0:T(8,128)(2,1)}), bf16[16,48,2048]{2,1,0:T(8,128)(2,1)}, u32[]{:S(2)}, u32[]{:S(2)}) async-start(bf16[16,48,2048]{2,1,0:T(8,128)(2,1)} %bitcast.35), calls=%async_computation | async-start | bytes 6291456 | tf_op jit(solution)/shard_map/all_to_all | solution.py:361
  202.5 3.8 %copy-start.5 = (f32[2048]{0:T(1024)S(1)}, f32[2048]{0:T(1024)}, u32[]{:S(2)}) copy-start(f32[2048]{0:T(1024)} %param.33) | copy-start | bytes 24580
  202.5 3.8 %copy-start.6 = (f32[2048]{0:T(1024)S(1)}, f32[2048]{0:T(1024)}, u32[]{:S(2)}) copy-start(f32[2048]{0:T(1024)} %param.32) | copy-start | bytes 24580

commit v4 on v3

--- a/solution.py
+++ b/solution.py
@@ -48,6 +48,8 @@
     weight_recv,
     part_send,
     part_recv,
+    pass_send,
+    pass_recv,
     own_sem,
 ):
     mesh_ids = pl.DeviceIdType.MESH
@@ -109,15 +111,63 @@
             device_id_type=mesh_ids,
         )
 
-    def weight_copy(step, landing):
+    pair, side = tp_index // 2, lax.rem(tp_index, 2)
+    pairs = n_tp // 2
+    half = weight_ref.shape[0] // 2
+    sibling = tp_index + 1 - 2 * side
+
+    def sibling_copy(landing):
         return pltpu.make_async_remote_copy(
             src_ref=weight_ref,
             dst_ref=weights_ref.at[landing],
-            send_sem=weight_send.at[step],
-            recv_sem=weight_recv.at[step],
-            device_id={"tp": lax.rem(tp_index + step, n_tp)},
-            device_id_type=mesh_ids,
-        )
+            send_sem=weight_send.at[0],
+            recv_sem=weight_recv.at[0],
+            device_id={"tp": sibling},
+            device_id_type=mesh_ids,
+        )
+
+    def half_rows(which):
+        return pl.ds(pl.multiple_of(which * half, half), half)
+
+    def slot(step, which):
+        return 1 + (step - 1) * 2 + which
+
+    def half_send(step, which):
+        target = lax.rem(pair + step, pairs) * 2 + which
+        return pltpu.make_async_remote_copy(
+            src_ref=weight_ref.at[half_rows(which)],
+            dst_ref=weights_ref.at[tp_index, half_rows(which)],
+            send_sem=weight_send.at[slot(step, which)],
+            recv_sem=weight_recv.at[slot(step, side)],
+            device_id={"tp": target},
+            device_id_type=mesh_ids,
+        )
+
+    def half_arrived(step, which):
+        source = lax.rem(pair + pairs - step, pairs) * 2 + which
+        place = weights_ref.at[source, half_rows(side)]
+        return pltpu.make_async_remote_copy(
+            src_ref=place,
+            dst_ref=place,
+            send_sem=weight_send.at[slot(step, which)],
+            recv_sem=weight_recv.at[slot(step, which)],
+            device_id={"tp": source},
+            device_id_type=mesh_ids,
+        )
+
+    def half_pass(step, which, part):
+        source = lax.rem(pair + pairs - step, pairs) * 2 + which
+        place = weights_ref.at[source, half_rows(part)]
+        return pltpu.make_async_remote_copy(
+            src_ref=place,
+            dst_ref=place,
+            send_sem=pass_send.at[slot(step, which)],
+            recv_sem=pass_recv.at[slot(step, which)],
+            device_id={"tp": sibling},
+            device_id_type=mesh_ids,
+        )
+
+    others = [(step, which) for step in range(1, pairs) for which in range(2)]
 
     def part_copy(step, landing):
         peer = lax.rem(tp_index + step, n_tp)
@@ -138,8 +188,9 @@
         for which in range(2):
             held_copy(0, which).start()
 
-    for step in range(1, n_tp):
-        weight_copy(step, tp_index).start()
+    for step, which in others:
+        half_send(step, which).start()
+    sibling_copy(tp_index).start()
 
     key_lane = lax.broadcasted_iota(jnp.int32, (tile, KBLK), 1)
     query_row = lax.broadcasted_iota(jnp.int32, (tile, KBLK), 0)
@@ -195,6 +246,9 @@
     for step in range(1, n_tp):
         part_copy(step, tp_index).start()
     parts_ref[tp_index] = ready[tp_index]
+    for step, which in others:
+        half_arrived(step, which).wait_recv()
+        half_pass(step, which, side).start()
 
     @pl.when(has_next)
     def _():
@@ -205,8 +259,13 @@
 
     for step in range(1, n_tp):
         source = lax.rem(tp_index + n_tp - step, n_tp)
-        weight_copy(step, source).wait()
         part_copy(step, source).wait()
+    for step, which in others:
+        half_send(step, which).wait_send()
+        half_pass(step, which, side).wait_send()
+        half_pass(step, which, 1 - side).wait_recv()
+    sibling_copy(tp_index).wait_send()
+    sibling_copy(sibling).wait_recv()
 
 
 def mixer(query_rows, key_rows, value_rows, output_weight):
@@ -231,6 +290,8 @@
             pltpu.VMEM((n_tp, tokens, features), jnp.bfloat16),
             dma((n_sp, 2)),
             dma((n_sp, 2)),
+            dma((n_tp,)),
+            dma((n_tp,)),
             dma((n_tp,)),
             dma((n_tp,)),
             dma((n_tp,)),
@@ -371,7 +432,9 @@
     gate_act = jnp.dot(normed, shared_gate, preferred_element_type=jnp.float32)
     up_act = jnp.dot(normed, shared_up, preferred_element_type=jnp.float32)
     shared_hidden = (jax.nn.silu(gate_act) * up_act).astype(jnp.bfloat16)
-    shared_out = jnp.dot(shared_hidden, shared_down, preferred_element_type=jnp.float32)
+    shared_out = lax.optimization_barrier(
+        jnp.dot(shared_hidden, shared_down, preferred_element_type=jnp.float32)
+    )
     final = layer_norm(normed.astype(jnp.float32) + routed + shared_out, second_gain, second_bias)
     return final.astype(jnp.bfloat16)
 

time: 208 us -> 204 us (0.981)
  waiting for transfers between devices: 67.7 us -> 63.9 us
    pallas_call x1, Pallas kernels: 72.9 us -> 83.5 us  [exchange(): pl.pallas_call(functools.partial(exchange_kernel, n_sp, n_tp), out_shape=...]
    pallas_call x1, Pallas kernels: 30 us -> 19.6 us  [mixer(): pl.pallas_call(functools.partial(mixer_kernel, n_sp, n_tp), out_shape=(ja...]
    all_to_all x1, waiting for transfers between devices: 67.7 us -> 63.9 us  [local(): lax.all_to_all(results, ('sp', 'tp'), split_axis=0, concat_axis=0, tiled=...]
  transfers between devices with their start and end apart: 1 -> 1, of which waited for: 1 -> 1; matrix products, arithmetic and copies ran while one was open for 1% -> 3% of each run, Pallas kernels for 0% -> 0%
where the time goes in v4:
time: 204 us; the launch traced here: 203 us
  Pallas kernels  103 us (50%)
  waiting for transfers between devices  63.9 us (31%)
  matrix products  25.7 us (13%)
  starting transfers between devices  5.6 us (3%)
  other arithmetic  2.84 us (1%)
  local copies, waits for them, and re-layouts  2.05 us (1%)
    pallas_call x1, Pallas kernels, exchange(): pl.pallas_call(functools.partial(exchange_kernel, n_sp, n_tp), out_shape=...  83.5 us
    all_to_all x1, waiting for transfers between devices, local(): lax.all_to_all(results, ('sp', 'tp'), split_axis=0, concat_axis=0, tiled=...  63.9 us
    pallas_call x1, Pallas kernels, mixer(): pl.pallas_call(functools.partial(mixer_kernel, n_sp, n_tp), out_shape=(ja...  19.6 us
    dot_general x1, matrix products, local(): jnp.dot(hidden, down_weight[0], preferred_element_type=jnp.float32)  7.72 us
    all_to_all x1, starting transfers between devices, local(): lax.all_to_all(results, ('sp', 'tp'), split_axis=0, concat_axis=0, tiled=...  5.6 us
  transfers between devices with their start and end apart: 1, of which 1 were waited for; matrix products, arithmetic and copies ran while one was open for 3% of the time, Pallas kernels for 0%

profile of v4, /device:TPU:11, one launch (start us, length us, event | category | flops | bytes accessed | tf_op | source)
XLA Modules:
  0.0 203.3 jit_solution(15038853782798670133)
XLA Ops:
  0.0 19.6 %shard_map.163 = (bf16[4,128,128]{2,1,0:T(8,128)(2,1)}, bf16[4,128,2048]{2,1,0:T(8,128)(2,1)}) custom-call(bf16[512,128]{1,0:T(8,128)(2,1)} %query_ref.1, bf16[512,128]{1,0:T(8,128)(2,1)} %key_ref.1, bf16[512,128]{1,0:T(8,128)(2,1)} %value_ref.1, bf16[128,2048]{1,0:T(8,128)(2,1)} %weight_ref.1), custom_call_target="tpu_custom_call" | custom-call | tf_op jit(solution)/shard_map/pallas_call | solution.py:278
  19.6 0.8 slice_bitcast_fusion.3
  20.4 0.0 copy-start.7
  20.4 0.0 copy-start.3
  20.5 0.0 copy-start.4
  20.5 2.2 %fusion.44 = (f32[128]{0:T(128)S(1)}, f32[128,2048]{1,0:T(8,128)S(1)}) fusion(bf16[512,2048]{1,0:T(8,128)(2,1)} %bitcast.38, bf16[128,128]{1,0:T(8,128)(2,1)S(1)} %get-tuple-element.14, bf16[128,128]{1,0:T(8,128)(2,1)S(1)} %get-tuple-element.15, bf16[128,128]{1,0:T(8,128)(2,1)S(1)} %get-tuple-element.16, bf16[128,128]{1,0:T(8,128)(2,1)S(1)} %get-tuple-element.13, ...), kind=kOutput, calls=%fused_computation.69 | convolution fusion | flops 269746048 | bytes 3801600 | tf_op jit(solution)/shard_map/dot_general | solution.py:388
  22.7 0.3 multiply_reduce_fusion.1
  23.0 0.1 copy.30
  23.1 0.1 eq.20
  23.2 0.3 fusion.4
  23.5 0.1 convert_element_type.49
  23.6 0.1 copy.31
  23.7 0.2 fusion
  23.9 0.2 add_convert_fusion.1
  24.2 0.0 copy-start.1
  24.2 0.8 copy-done.1
  25.0 2.6 %convolution_convert_fusion.1 = bf16[768,2048]{1,0:T(8,128)(2,1)} fusion(pred[768,128]{1,0:T(8,128)(4,1)S(1)} %fusion, bf16[128,2048]{1,0:T(8,128)(2,1)S(1)} %add_convert_fusion.1), kind=kOutput, calls=%fused_computation.1 | convolution fusion | flops 404226048 | bytes 3768320 | tf_op jit(solution)/shard_map/dot_general | solution.py:411
  27.6 83.5 %shard_map.164 = bf16[16,48,2048]{2,1,0:T(8,128)(2,1)} custom-call(bf16[16,48,2048]{2,1,0:T(8,128)(2,1)} %bitcast.34), custom_call_target="tpu_custom_call" | custom-call | tf_op jit(solution)/shard_map/pallas_call | solution.py:350
  111.1 4.0 %fusion.10 = f32[768,256]{1,0:T(8,128)} fusion(bf16[768,2048]{1,0:T(8,128)(2,1)} %bitcast.36, bf16[1,2048,256]{2,1,0:T(8,128)(2,1)} %param.26), kind=kOutput, calls=%fused_computation.19 | convolution fusion | flops 805306368 | bytes 4980736 | tf_op jit(solution)/shard_map/dot_general | solution.py:415
  115.1 7.7 %convolution_convert_fusion = bf16[768,2048]{1,0:T(8,128)(2,1)} fusion(bf16[768,2048]{1,0:T(8,128)(2,1)} %bitcast.37, bf16[1,256,2048]{2,1,0:T(8,128)(2,1)} %param.28, bf16[1,2048,256]{2,1,0:T(8,128)(2,1)} %param.27, f32[768,256]{1,0:T(8,128)} %fusion.10), kind=kOutput, calls=%fused_computation | convolution fusion | flops 1613365248 | bytes 9175040 | tf_op jit(solution)/shard_map/dot_general | solution.py:418
  122.8 5.6 %all-to-all-start = ((bf16[16,48,2048]{2,1,0:T(8,128)(2,1)}), bf16[16,48,2048]{2,1,0:T(8,128)(2,1)}, u32[]{:S(2)}, u32[]{:S(2)}) async-start(bf16[16,48,2048]{2,1,0:T(8,128)(2,1)} %bitcast.35), calls=%async_computation | async-start | bytes 6291456 | tf_op jit(solution)/shard_map/all_to_all | solution.py:422
  128.5 2.2 %fusion.45 = f32[128,512]{1,0:T(8,128)S(1)} fusion(bf16[128,2048]{1,0:T(8,128)(2,1)} %copy-done.1, bf16[2048,512]{1,0:T(8,128)(2,1)} %param.29), kind=kOutput, calls=%fused_computation.70 | convolution fusion | flops 268435456 | bytes 2883584 | tf_op jit(solution)/shard_map/dot_general | solution.py:432
  130.7 0.0 copy-start.10
  130.7 3.6 %fusion.3 = f32[128,2048]{1,0:T(8,128)} fusion(bf16[512,2048]{1,0:T(8,128)(2,1)S(1)} %copy-done, bf16[128,2048]{1,0:T(8,128)(2,1)} %copy-done.1, bf16[2048,512]{1,0:T(8,128)(2,1)} %param.30, f32[128,512]{1,0:T(8,128)S(1)} %fusion.45), kind=kOutput, calls=%fused_computation.11 | convolution fusion | flops 537264128 | bytes 6029312 | tf_op jit(solution)/shard_map/dot_general | solution.py:436
  134.3 0.2 select_reduce_fusion
  134.6 63.9 %all-to-all-done = bf16[16,48,2048]{2,1,0:T(8,128)(2,1)} async-done(((bf16[16,48,2048]{2,1,0:T(8,128)(2,1)}), bf16[16,48,2048]{2,1,0:T(8,128)(2,1)}, u32[]{:S(2)}, u32[]{:S(2)}) %all-to-all-start) | async-done | bytes 3145760 | tf_op jit(solution)/shard_map/all_to_all | solution.py:422
  198.5 3.0 %fusion.18 = f32[256,2048]{1,0:T(8,128)S(1)} fusion(bf16[768,2048]{1,0:T(8,128)(2,1)} %bitcast.11, bf16[128,768]{1,0:T(8,128)(2,1)S(1)} %get-tuple-element.12, bf16[128,768]{1,0:T(8,128)(2,1)S(1)} %get-tuple-element.11), kind=kOutput, calls=%fused_computation.34 | convolution fusion | flops 806092800 | bytes 5636096 | tf_op jit(solution)/shard_map/dot_general | solution.py:430
  201.4 0.0 copy-start.5
  201.5 0.0 copy-start.6
  201.5 0.5 fusion.42
  202.0 0.3 multiply_reduce_fusion
  202.3 1.0 add_convert_fusion
  (25 shorter events, 0.1 us)
Async XLA Ops:
  0.0 130.7 %copy-start = (bf16[512,2048]{1,0:T(8,128)(2,1)S(1)}, bf16[512,2048]{1,0:T(8,128)(2,1)}, u32[]{:S(2)}) copy-start(bf16[512,2048]{1,0:T(8,128)(2,1)} %param.31) | copy-start | bytes 6291460
  20.4 2.5 %copy-start.7 = (s32[128,4]{0,1:T(4,128)S(1)}, s32[128,4]{0,1:T(4,128)}, u32[]{:S(2)}) copy-start(s32[128,4]{0,1:T(4,128)} %param.24) | copy-start | bytes 6148
  20.4 3.5 %copy-start.3 = (f32[2048]{0:T(1024)S(1)}, f32[2048]{0:T(1024)}, u32[]{:S(2)}) copy-start(f32[2048]{0:T(1024)} %param.23) | copy-start | bytes 24580
  20.5 3.5 %copy-start.4 = (f32[2048]{0:T(1024)S(1)}, f32[2048]{0:T(1024)}, u32[]{:S(2)}) copy-start(f32[2048]{0:T(1024)} %param.22) | copy-start | bytes 24580
  22.7 4.9 %copy-start.8 = (f32[128]{0:T(128)}, f32[128]{0:T(128)S(1)}, u32[]{:S(2)}) copy-start(f32[128]{0:T(128)S(1)} %broadcast_multiply_fusion.1) | copy-start | bytes 1540
  23.0 4.6 %copy-start.11 = (f32[128]{0:T(128)}, f32[128]{0:T(128)S(1)}, u32[]{:S(2)}) copy-start(f32[128]{0:T(128)S(1)} %add_rsqrt_fusion.1) | copy-start | bytes 1540
  24.2 0.8 copy-start.1
  122.8 75.6 %all-to-all-start = ((bf16[16,48,2048]{2,1,0:T(8,128)(2,1)}), bf16[16,48,2048]{2,1,0:T(8,128)(2,1)}, u32[]{:S(2)}, u32[]{:S(2)}) async-start(bf16[16,48,2048]{2,1,0:T(8,128)(2,1)} %bitcast.35), calls=%async_computation | async-start | bytes 6291456 | tf_op jit(solution)/shard_map/all_to_all | solution.py:422
  130.7 3.6 %copy-start.10 = (f32[128,4]{0,1:T(4,128)S(1)}, f32[128,4]{0,1:T(4,128)}, u32[]{:S(2)}) copy-start(f32[128,4]{0,1:T(4,128)} %param.25) | copy-start | bytes 6148
  198.4 3.0 %copy-start.2 = (f32[128,2048]{1,0:T(8,128)S(1)}, f32[128,2048]{1,0:T(8,128)}, u32[]{:S(2)}) copy-start(f32[128,2048]{1,0:T(8,128)} %fusion.3) | copy-start | bytes 3145732
  198.4 3.0 %copy-start.9 = (f32[128]{0:T(128)S(1)}, f32[128]{0:T(128)}, u32[]{:S(2)}) copy-start(f32[128]{0:T(128)} %copy-done.8) | copy-start | bytes 1540
  198.5 3.0 %copy-start.12 = (f32[128]{0:T(128)S(1)}, f32[128]{0:T(128)}, u32[]{:S(2)}) copy-start(f32[128]{0:T(128)} %copy-done.11) | copy-start | bytes 1540
  201.4 0.8 copy-start.5
  201.5 0.8 copy-start.6

commit v5 on v4

--- a/solution.py
+++ b/solution.py
@@ -199,25 +199,16 @@
     reach = ((from_row >= to_lane) | (to_lane >= KBLK)).astype(jnp.float32).astype(jnp.bfloat16)
     reach = jnp.concatenate([reach, reach, reach], axis=0)
 
-    @pl.loop(0, seq_index + 1)
-    def _(step):
-        @pl.when(step > 0)
-        def _():
-            for which in range(2):
-                arrived(step, which).wait_recv()
-
-            @pl.when(has_next)
-            def _():
-                for which in range(2):
-                    held_copy(step, which).start()
-
-        block = seq_index - step
+    def visit(block, diagonal):
         for head in range(heads):
             lanes = slice(head * HEAD_DIM, (head + 1) * HEAD_DIM)
             for first_key in reversed(range(0, shard_len, KBLK)):
                 key_block = held[block, 0, first_key : first_key + KBLK, lanes]
                 value_block = held[block, 1, first_key : first_key + KBLK, lanes]
                 for first_query in range(0, shard_len, tile):
+                    if diagonal and first_key >= first_query + tile:
+                        continue
+                    masked = diagonal and first_key + KBLK > first_query
                     rows = slice(first_query, first_query + tile)
                     score = scale * lax.dot_general(
                         query_ref[rows, lanes],
@@ -225,13 +216,14 @@
                         (((1,), (1,)), ((), ())),
                         preferred_element_type=jnp.float32,
                     )
-                    usable = (key_lane + first_key) < (
-                        query_row + (first_query + step * shard_len)
-                    )
-                    grown = jnp.maximum(score, 0.0) + jnp.log(1.0 + jnp.exp(-jnp.abs(score)))
-                    spent = jnp.where(usable, grown, 0.0)
+                    usable = (key_lane + first_key) < (query_row + first_query)
+                    spent = jnp.maximum(score, 0.0) + jnp.log(1.0 + jnp.exp(-jnp.abs(score)))
+                    if masked:
+                        spent = jnp.where(usable, spent, 0.0)
                     sums = jnp.dot(three_parts(spent), reach, preferred_element_type=jnp.float32)
-                    share = jnp.where(usable, jnp.exp(score - sums[:, :KBLK]), 0.0)
+                    share = jnp.exp(score - sums[:, :KBLK])
+                    if masked:
+                        share = jnp.where(usable, share, 0.0)
                     piece = jnp.dot(
                         share.astype(jnp.bfloat16),
                         value_block,
@@ -240,6 +232,20 @@
                     before = behind[head, rows, :]
                     summed[rows, lanes] += piece * jnp.exp(-before)
                     behind[head, rows, :] = before + sums[:, KBLK:]
+
+    visit(seq_index, True)
+
+    @pl.loop(1, seq_index + 1)
+    def _(step):
+        for which in range(2):
+            arrived(step, which).wait_recv()
+
+        @pl.when(has_next)
+        def _():
+            for which in range(2):
+                held_copy(step, which).start()
+
+        visit(seq_index - step, False)
 
     for peer in range(n_tp):
         ready[peer] = summed[peer * tokens : (peer + 1) * tokens, :].astype(jnp.bfloat16)

time: 204 us -> 204 us (level)
  no operation moved by 1% of the time
where the time goes in v5:
time: 204 us; the launch traced here: 203 us
  Pallas kernels  103 us (50%)
  waiting for transfers between devices  63.9 us (31%)
  matrix products  25.7 us (13%)
  starting transfers between devices  5.61 us (3%)
  other arithmetic  2.84 us (1%)
  local copies, waits for them, and re-layouts  2.05 us (1%)
    pallas_call x1, Pallas kernels, exchange(): pl.pallas_call(functools.partial(exchange_kernel, n_sp, n_tp), out_shape=...  83.3 us
    all_to_all x1, waiting for transfers between devices, local(): lax.all_to_all(results, ('sp', 'tp'), split_axis=0, concat_axis=0, tiled=...  63.9 us
    pallas_call x1, Pallas kernels, mixer(): pl.pallas_call(functools.partial(mixer_kernel, n_sp, n_tp), out_shape=(ja...  19.6 us
    dot_general x1, matrix products, local(): jnp.dot(hidden, down_weight[0], preferred_element_type=jnp.float32)  7.72 us
    all_to_all x1, starting transfers between devices, local(): lax.all_to_all(results, ('sp', 'tp'), split_axis=0, concat_axis=0, tiled=...  5.61 us
  transfers between devices with their start and end apart: 1, of which 1 were waited for; matrix products, arithmetic and copies ran while one was open for 3% of the time, Pallas kernels for 0%

profile of v5, /device:TPU:11, one launch (start us, length us, event | category | flops | bytes accessed | tf_op | source)
XLA Modules:
  0.0 203.2 jit_solution(312848721057533473)
XLA Ops:
  0.0 19.6 %shard_map.163 = (bf16[4,128,128]{2,1,0:T(8,128)(2,1)}, bf16[4,128,2048]{2,1,0:T(8,128)(2,1)}) custom-call(bf16[512,128]{1,0:T(8,128)(2,1)} %query_ref.1, bf16[512,128]{1,0:T(8,128)(2,1)} %key_ref.1, bf16[512,128]{1,0:T(8,128)(2,1)} %value_ref.1, bf16[128,2048]{1,0:T(8,128)(2,1)} %weight_ref.1), custom_call_target="tpu_custom_call" | custom-call | tf_op jit(solution)/shard_map/pallas_call | solution.py:284
  19.6 0.8 slice_bitcast_fusion.3
  20.4 0.0 copy-start.7
  20.4 0.0 copy-start.3
  20.4 0.0 copy-start.4
  20.5 2.2 %fusion.44 = (f32[128]{0:T(128)S(1)}, f32[128,2048]{1,0:T(8,128)S(1)}) fusion(bf16[512,2048]{1,0:T(8,128)(2,1)} %bitcast.38, bf16[128,128]{1,0:T(8,128)(2,1)S(1)} %get-tuple-element.14, bf16[128,128]{1,0:T(8,128)(2,1)S(1)} %get-tuple-element.15, bf16[128,128]{1,0:T(8,128)(2,1)S(1)} %get-tuple-element.16, bf16[128,128]{1,0:T(8,128)(2,1)S(1)} %get-tuple-element.13, ...), kind=kOutput, calls=%fused_computation.69 | convolution fusion | flops 269746048 | bytes 3801600 | tf_op jit(solution)/shard_map/dot_general | solution.py:394
  22.7 0.3 multiply_reduce_fusion.1
  23.0 0.1 copy.30
  23.1 0.1 eq.20
  23.2 0.3 fusion.4
  23.5 0.1 convert_element_type.49
  23.6 0.1 copy.31
  23.7 0.2 fusion
  23.9 0.2 add_convert_fusion.1
  24.2 0.0 copy-start.1
  24.2 0.8 copy-done.1
  25.0 2.6 %convolution_convert_fusion.1 = bf16[768,2048]{1,0:T(8,128)(2,1)} fusion(pred[768,128]{1,0:T(8,128)(4,1)S(1)} %fusion, bf16[128,2048]{1,0:T(8,128)(2,1)S(1)} %add_convert_fusion.1), kind=kOutput, calls=%fused_computation.1 | convolution fusion | flops 404226048 | bytes 3768320 | tf_op jit(solution)/shard_map/dot_general | solution.py:417
  27.6 83.3 %shard_map.164 = bf16[16,48,2048]{2,1,0:T(8,128)(2,1)} custom-call(bf16[16,48,2048]{2,1,0:T(8,128)(2,1)} %bitcast.34), custom_call_target="tpu_custom_call" | custom-call | tf_op jit(solution)/shard_map/pallas_call | solution.py:356
  111.0 4.0 %fusion.10 = f32[768,256]{1,0:T(8,128)} fusion(bf16[768,2048]{1,0:T(8,128)(2,1)} %bitcast.36, bf16[1,2048,256]{2,1,0:T(8,128)(2,1)} %param.26), kind=kOutput, calls=%fused_computation.19 | convolution fusion | flops 805306368 | bytes 4980736 | tf_op jit(solution)/shard_map/dot_general | solution.py:421
  115.0 7.7 %convolution_convert_fusion = bf16[768,2048]{1,0:T(8,128)(2,1)} fusion(bf16[768,2048]{1,0:T(8,128)(2,1)} %bitcast.37, bf16[1,256,2048]{2,1,0:T(8,128)(2,1)} %param.28, bf16[1,2048,256]{2,1,0:T(8,128)(2,1)} %param.27, f32[768,256]{1,0:T(8,128)} %fusion.10), kind=kOutput, calls=%fused_computation | convolution fusion | flops 1613365248 | bytes 9175040 | tf_op jit(solution)/shard_map/dot_general | solution.py:424
  122.7 5.6 %all-to-all-start = ((bf16[16,48,2048]{2,1,0:T(8,128)(2,1)}), bf16[16,48,2048]{2,1,0:T(8,128)(2,1)}, u32[]{:S(2)}, u32[]{:S(2)}) async-start(bf16[16,48,2048]{2,1,0:T(8,128)(2,1)} %bitcast.35), calls=%async_computation | async-start | bytes 6291456 | tf_op jit(solution)/shard_map/all_to_all | solution.py:428
  128.3 2.2 %fusion.45 = f32[128,512]{1,0:T(8,128)S(1)} fusion(bf16[128,2048]{1,0:T(8,128)(2,1)} %copy-done.1, bf16[2048,512]{1,0:T(8,128)(2,1)} %param.29), kind=kOutput, calls=%fused_computation.70 | convolution fusion | flops 268435456 | bytes 2883584 | tf_op jit(solution)/shard_map/dot_general | solution.py:438
  130.6 0.0 copy-start.10
  130.6 3.6 %fusion.3 = f32[128,2048]{1,0:T(8,128)} fusion(bf16[512,2048]{1,0:T(8,128)(2,1)S(1)} %copy-done, bf16[128,2048]{1,0:T(8,128)(2,1)} %copy-done.1, bf16[2048,512]{1,0:T(8,128)(2,1)} %param.30, f32[128,512]{1,0:T(8,128)S(1)} %fusion.45), kind=kOutput, calls=%fused_computation.11 | convolution fusion | flops 537264128 | bytes 6029312 | tf_op jit(solution)/shard_map/dot_general | solution.py:442
  134.2 0.2 select_reduce_fusion
  134.5 63.9 %all-to-all-done = bf16[16,48,2048]{2,1,0:T(8,128)(2,1)} async-done(((bf16[16,48,2048]{2,1,0:T(8,128)(2,1)}), bf16[16,48,2048]{2,1,0:T(8,128)(2,1)}, u32[]{:S(2)}, u32[]{:S(2)}) %all-to-all-start) | async-done | bytes 3145760 | tf_op jit(solution)/shard_map/all_to_all | solution.py:428
  198.3 3.0 %fusion.18 = f32[256,2048]{1,0:T(8,128)S(1)} fusion(bf16[768,2048]{1,0:T(8,128)(2,1)} %bitcast.11, bf16[128,768]{1,0:T(8,128)(2,1)S(1)} %get-tuple-element.12, bf16[128,768]{1,0:T(8,128)(2,1)S(1)} %get-tuple-element.11), kind=kOutput, calls=%fused_computation.34 | convolution fusion | flops 806092800 | bytes 5636096 | tf_op jit(solution)/shard_map/dot_general | solution.py:436
  201.3 0.0 copy-start.5
  201.3 0.0 copy-start.6
  201.3 0.5 fusion.42
  201.9 0.3 multiply_reduce_fusion
  202.1 1.0 add_convert_fusion
  (25 shorter events, 0.1 us)
Async XLA Ops:
  0.0 130.6 %copy-start = (bf16[512,2048]{1,0:T(8,128)(2,1)S(1)}, bf16[512,2048]{1,0:T(8,128)(2,1)}, u32[]{:S(2)}) copy-start(bf16[512,2048]{1,0:T(8,128)(2,1)} %param.31) | copy-start | bytes 6291460
  20.4 2.5 %copy-start.7 = (s32[128,4]{0,1:T(4,128)S(1)}, s32[128,4]{0,1:T(4,128)}, u32[]{:S(2)}) copy-start(s32[128,4]{0,1:T(4,128)} %param.24) | copy-start | bytes 6148
  20.4 3.5 %copy-start.3 = (f32[2048]{0:T(1024)S(1)}, f32[2048]{0:T(1024)}, u32[]{:S(2)}) copy-start(f32[2048]{0:T(1024)} %param.23) | copy-start | bytes 24580
  20.4 3.5 %copy-start.4 = (f32[2048]{0:T(1024)S(1)}, f32[2048]{0:T(1024)}, u32[]{:S(2)}) copy-start(f32[2048]{0:T(1024)} %param.22) | copy-start | bytes 24580
  22.7 4.9 %copy-start.8 = (f32[128]{0:T(128)}, f32[128]{0:T(128)S(1)}, u32[]{:S(2)}) copy-start(f32[128]{0:T(128)S(1)} %broadcast_multiply_fusion.1) | copy-start | bytes 1540
  23.0 4.6 %copy-start.11 = (f32[128]{0:T(128)}, f32[128]{0:T(128)S(1)}, u32[]{:S(2)}) copy-start(f32[128]{0:T(128)S(1)} %add_rsqrt_fusion.1) | copy-start | bytes 1540
  24.2 0.8 copy-start.1
  122.7 75.6 %all-to-all-start = ((bf16[16,48,2048]{2,1,0:T(8,128)(2,1)}), bf16[16,48,2048]{2,1,0:T(8,128)(2,1)}, u32[]{:S(2)}, u32[]{:S(2)}) async-start(bf16[16,48,2048]{2,1,0:T(8,128)(2,1)} %bitcast.35), calls=%async_computation | async-start | bytes 6291456 | tf_op jit(solution)/shard_map/all_to_all | solution.py:428
  130.6 3.6 %copy-start.10 = (f32[128,4]{0,1:T(4,128)S(1)}, f32[128,4]{0,1:T(4,128)}, u32[]{:S(2)}) copy-start(f32[128,4]{0,1:T(4,128)} %param.25) | copy-start | bytes 6148
  198.3 3.0 %copy-start.2 = (f32[128,2048]{1,0:T(8,128)S(1)}, f32[128,2048]{1,0:T(8,128)}, u32[]{:S(2)}) copy-start(f32[128,2048]{1,0:T(8,128)} %fusion.3) | copy-start | bytes 3145732
  198.3 3.0 %copy-start.9 = (f32[128]{0:T(128)S(1)}, f32[128]{0:T(128)}, u32[]{:S(2)}) copy-start(f32[128]{0:T(128)} %copy-done.8) | copy-start | bytes 1540
  198.3 3.0 %copy-start.12 = (f32[128]{0:T(128)S(1)}, f32[128]{0:T(128)}, u32[]{:S(2)}) copy-start(f32[128]{0:T(128)} %copy-done.11) | copy-start | bytes 1540
  201.3 0.8 copy-start.5
  201.3 0.8 copy-start.6
